TPU v7x, 32 devices: a whole 2x2x4 slice. The times are simulated.
32 devices in a mesh: sp: 4 (over y, x), tp: 8 (over z, core).
Axes of the slice: x: 2, y: 2, z: 4, core: 2. Of those that a mesh axis runs over, the one named last changes fastest.
Arguments:
- queries: bfloat16 [1536, 2048], P('sp', 'tp'), may hold values from -6 to 6
- keys: bfloat16 [1536, 2048], P('sp', 'tp'), may hold values from -6 to 6
- values: bfloat16 [1536, 2048], P('sp', 'tp'), may hold values from -6 to 6
- key_bias: bfloat16 [1536, 32], P('sp', 'tp'), may hold values from -16 to 0
- head_gain: float32 [32, 64], P('tp'), may hold values from 0.1 to 1.9
- out_weight: bfloat16 [2048, 2048], P('tp'), may hold values from -0.125 to 0.125
- residual: bfloat16 [1536, 2048], P(('sp', 'tp')), may hold values from -6 to 6
- norm_gain: float32 [2048], replicated, may hold values from 0.1 to 1.9
- gate_proj: bfloat16 [4, 2048, 7168], P('sp', None, 'tp'), may hold values from -0.125 to 0.125
- up_proj: bfloat16 [4, 2048, 7168], P('sp', None, 'tp'), may hold values from -0.125 to 0.125
- down_proj: bfloat16 [4, 7168, 2048], P('sp', 'tp'), may hold values from -0.0625 to 0.0625
- expert_choice: int32 [1536, 2], P(('sp', 'tp')), may hold values from 0 to 3, all different within a row; in each aligned block of 48 rows (0 to 47, 48 to 95, ...) at most 48 rows name the same one
- expert_weights: float32 [1536, 2], P(('sp', 'tp')), may hold values from 0.2 to 1
Outputs:
- layer_out: bfloat16 [1536, 2048], P(('sp', 'tp'))
Inputs may be any that keep to these rules, and one draw needn't show every extreme that they name: `expert_choice`: in each aligned block of 48 rows (the rows of one device), no expert is named more than 48 times; the two experts of a row differ.
All inputs are finite; a program needn't handle non-finite values.
Results may differ from a plain program's by a relative error of at most 0.019.
Values may be sent and summed in bfloat16 or wider, within the bound.
A program may use at most 128 MiB of HBM per device.

v0:
```python
import functools

import jax
import jax.numpy as jnp
from jax import lax
from jax.experimental import pallas as pl
from jax.experimental.pallas import tpu as pltpu
from jax.sharding import PartitionSpec as P

epsilon = 1e-06


def rms_scaled(values_in):
    return values_in * lax.rsqrt(jnp.mean(values_in * values_in, axis=-1, keepdims=True) + epsilon)


def expert_partial(row_block, gate_matrix, up_matrix, down_matrix):
    gate_part = jnp.dot(row_block, gate_matrix, preferred_element_type=jnp.float32)
    up_part = jnp.dot(row_block, up_matrix, preferred_element_type=jnp.float32)
    hidden = (jax.nn.silu(gate_part) * up_part).astype(jnp.bfloat16)
    return jnp.dot(hidden, down_matrix, preferred_element_type=jnp.float32)


def choice_ranks(routes, experts_all):
    flat_routes = routes.reshape(routes.shape[:-2] + (-1,))
    onehot = (flat_routes[..., None] == jnp.arange(experts_all, dtype=jnp.int32)).astype(jnp.int32)
    before = jnp.cumsum(onehot, axis=-2) - onehot
    return jnp.sum(before * onehot, axis=-1).reshape(routes.shape)


def slot_tokens(slot_index, targets, missing):
    flat_slots = slot_index.reshape(-1)
    owners = jnp.arange(flat_slots.shape[0], dtype=jnp.int32) // 2
    matches = flat_slots[None, :] == jnp.arange(targets, dtype=jnp.int32)[:, None]
    owner_found = jnp.sum(jnp.where(matches, owners[None, :], 0), axis=1)
    return jnp.where(jnp.any(matches, axis=1), owner_found, missing)


def softplus_parts(scores):
    drops = -jnp.maximum(scores, 0.0) - jnp.log(1.0 + jnp.exp(-jnp.abs(scores)))
    return drops, scores + drops


def attend_block(query_ref, key_of, value_of, bias_of, mix_ref, carry_ref, head_size, diagonal):
    rows, width = query_ref.shape
    lanes = 128 if width % 128 == 0 else width
    per_group = lanes // head_size
    chunk = 128 if rows % 128 == 0 else rows
    later_row = lax.broadcasted_iota(jnp.int32, (rows, rows), 0)
    later_col = lax.broadcasted_iota(jnp.int32, (rows, rows), 1)
    suffix_of = jnp.where(later_row > later_col, 1.0, 0.0).astype(jnp.bfloat16)
    lane_head = lax.broadcasted_iota(jnp.int32, (1, lanes), 1) // head_size
    for group in range(width // lanes):
        cols = slice(group * lanes, (group + 1) * lanes)
        key_tile = key_of(cols)
        value_tile = value_of(cols)
        for inner in range(per_group):
            mine = lane_head == inner
            bias_row = bias_of(group * per_group + inner)
            for start in range(0, rows, chunk):
                span = slice(start, start + chunk)
                query = query_ref[span, cols] * jnp.asarray(head_size**-0.5, jnp.bfloat16)
                query = jnp.where(mine, query, jnp.zeros_like(query))
                scores = lax.dot_general(
                    query, key_tile, (((1,), (1,)), ((), ())), preferred_element_type=jnp.float32
                )
                scores = scores + bias_row
                drops, hits = softplus_parts(scores)
                if diagonal:
                    row_pos = start + lax.broadcasted_iota(jnp.int32, (chunk, rows), 0)
                    col_pos = lax.broadcasted_iota(jnp.int32, (chunk, rows), 1)
                    earlier = col_pos < row_pos
                    drops = jnp.where(earlier, drops, 0.0)
                high = drops.astype(jnp.bfloat16)
                low = (drops - high.astype(jnp.float32)).astype(jnp.bfloat16)
                suffix = jnp.dot(high, suffix_of, preferred_element_type=jnp.float32)
                suffix = suffix + jnp.dot(low, suffix_of, preferred_element_type=jnp.float32)
                within = jnp.exp(hits + suffix)
                if diagonal:
                    within = jnp.where(earlier, within, 0.0)
                part = jnp.dot(
                    within.astype(jnp.bfloat16), value_tile, preferred_element_type=jnp.float32
                )
                total = suffix[:, 0:1] + drops[:, 0:1]
                if diagonal:
                    mix_old = jnp.zeros((chunk, lanes), jnp.float32)
                    carry_old = mix_old
                    if inner > 0:
                        mix_old = mix_ref[span, cols]
                        carry_old = carry_ref[span, cols]
                    mix_ref[span, cols] = jnp.where(mine, part, mix_old)
                    carry_ref[span, cols] = jnp.where(mine, total, carry_old)
                else:
                    mix_old = mix_ref[span, cols]
                    carry_old = carry_ref[span, cols]
                    mix_ref[span, cols] = jnp.where(
                        mine, mix_old + jnp.exp(carry_old) * part, mix_old
                    )
                    carry_ref[span, cols] = jnp.where(mine, carry_old + total, carry_old)


def diagonal_kernel(head_size, query_ref, key_ref, value_ref, bias_ref, mix_ref, carry_ref):
    attend_block(
        query_ref,
        lambda cols: key_ref[:, cols],
        lambda cols: value_ref[:, cols],
        lambda head: bias_ref[head : head + 1, :],
        mix_ref,
        carry_ref,
        head_size,
        True,
    )


def earlier_kernel(
    head_size, query_ref, pack_ref, bias_ref, mix_in, carry_in, gain_ref, out_ref, mix_ref, carry_ref
):
    rows, width = query_ref.shape
    lanes = 128 if width % 128 == 0 else width
    mix_ref[...] = mix_in[...]
    carry_ref[...] = carry_in[...]
    own = lax.axis_index("sp")

    def visit(step, nothing):
        block = own - 1 - step
        attend_block(
            query_ref,
            lambda cols: pack_ref[block, :rows, cols],
            lambda cols: pack_ref[block, :rows, slice(width + cols.start, width + cols.stop)],
            lambda head: bias_ref[block, head : head + 1, :],
            mix_ref,
            carry_ref,
            head_size,
            False,
        )
        return nothing

    lax.fori_loop(0, own, visit, 0)
    lane_head = lax.broadcasted_iota(jnp.int32, (1, lanes), 1) // head_size
    for group in range(width // lanes):
        cols = slice(group * lanes, (group + 1) * lanes)
        mixture = mix_ref[:, cols]
        squares = mixture * mixture
        scaled = mixture
        for inner in range(lanes // head_size):
            mine = lane_head == inner
            mean = jnp.sum(jnp.where(mine, squares, 0.0), axis=1, keepdims=True) / head_size
            scaled = jnp.where(mine, mixture * lax.rsqrt(mean + epsilon), scaled)
        out_ref[:, cols] = (scaled * gain_ref[:, cols]).astype(jnp.bfloat16)


def attention(queries, keys, values, key_bias, head_gain):
    rows, width = queries.shape
    heads, head_size = head_gain.shape
    blocks = lax.axis_size("sp")
    bias_own = key_bias.T
    extra = -(-heads * rows // (2 * width))
    padded = -(-(rows + extra) // 8) * 8 - rows
    flat_bias = jnp.pad(bias_own.reshape(-1), (0, padded * 2 * width - heads * rows))
    packed = jnp.concatenate(
        [jnp.concatenate([keys, values], axis=1), flat_bias.reshape(padded, 2 * width)], axis=0
    )
    gathered = lax.all_gather(packed, "sp", axis=0)
    vmem = pl.BlockSpec(memory_space=pltpu.VMEM)
    state = jax.ShapeDtypeStruct((rows, width), jnp.float32)
    work = heads * rows * rows
    mix, carry = pl.pallas_call(
        functools.partial(diagonal_kernel, head_size),
        out_shape=[state, state],
        in_specs=[vmem] * 4,
        out_specs=[vmem] * 2,
        cost_estimate=pl.CostEstimate(flops=work * 2000, bytes_accessed=10**6, transcendentals=0),
    )(queries, keys, values, bias_own.astype(jnp.float32))
    bias_all = gathered[:, rows:].reshape(blocks, -1)[:, : heads * rows]
    bias_all = bias_all.reshape(blocks, heads, rows).astype(jnp.float32)
    return pl.pallas_call(
        functools.partial(earlier_kernel, head_size),
        out_shape=jax.ShapeDtypeStruct((rows, width), jnp.bfloat16),
        in_specs=[vmem] * 6,
        out_specs=vmem,
        scratch_shapes=[pltpu.VMEM((rows, width), jnp.float32)] * 2,
        cost_estimate=pl.CostEstimate(flops=work * 4000, bytes_accessed=10**6, transcendentals=0),
    )(queries, gathered, bias_all, mix, carry, head_gain.reshape(1, width))


class Places:
    def __init__(self):
        self.sp = lax.axis_index("sp")
        self.tp = lax.axis_index("tp")
        self.depth = lax.axis_size("tp") // 2
        self.z = self.tp // 2
        self.core = self.tp % 2
        self.col = self.sp % 2
        self.line = self.sp // 2
        self.across = self.line * 2 + 1 - self.col
        self.along = (1 - self.line) * 2 + self.col
        self.far = (1 - self.line) * 2 + 1 - self.col
        self.partner = (self.sp, self.z * 2 + 1 - self.core)
        self.x_next = (self.across, self.tp)
        self.y_next = (self.along, self.tp)

    def z_peer(self, step):
        return lax.rem(self.z + step, self.depth)

    def z_device(self, step):
        return (self.sp, self.z_peer(step) * 2 + self.core)

    def meet(self, wide):
        barrier = pltpu.get_barrier_semaphore()
        peers = [self.partner] + [self.z_device(step) for step in range(1, self.depth)]
        if wide:
            peers = peers + [self.x_next, self.y_next]
        for peer in peers:
            pl.semaphore_signal(
                barrier, inc=1, device_id=peer, device_id_type=pl.DeviceIdType.MESH
            )
        pl.semaphore_wait(barrier, len(peers))


def remote(source, target, send_sem, recv_sem, device):
    return pltpu.make_async_remote_copy(
        src_ref=source,
        dst_ref=target,
        send_sem=send_sem,
        recv_sem=recv_sem,
        device_id=device,
        device_id_type=pl.DeviceIdType.MESH,
    )


def gather_kernel(own_ref, out_ref, local_sem, send_sems, recv_sems):
    place = Places()
    depth = place.depth
    place.meet(True)
    sends = []

    def slot(seq, z, core):
        return out_ref.at[seq, z, core]

    def send(source, seq, z, device, count):
        copy = remote(
            source,
            slot(seq, z, place.core),
            send_sems.at[count],
            recv_sems.at[seq, z, place.core],
            device,
        )
        copy.start()
        sends.append(copy)

    def arrived(seq, z, core):
        remote(
            own_ref, slot(seq, z, core), send_sems.at[0], recv_sems.at[seq, z, core], place.partner
        ).wait_recv()

    local = pltpu.make_async_copy(own_ref, slot(place.sp, place.z, place.core), local_sem)
    local.start()
    order = [0, 1] + list(range(depth - 1, 1, -1))
    for step in order[1:]:
        send(own_ref, place.sp, place.z, place.z_device(step), len(sends))
    for step in order:
        z = place.z_peer(step)
        source = own_ref
        if step > 0:
            arrived(place.sp, z, place.core)
            source = slot(place.sp, z, place.core)
        send(source, place.sp, z, place.x_next, len(sends))
        send(source, place.sp, z, place.y_next, len(sends))
        send(source, place.sp, z, place.partner, len(sends))
    for index, step in enumerate(order):
        z = place.z_peer(step)
        arrived(place.across, z, place.core)
        source = slot(place.across, z, place.core)
        if index % 2 == 0:
            send(source, place.across, z, place.y_next, len(sends))
        send(source, place.across, z, place.partner, len(sends))
        arrived(place.along, z, place.core)
        source = slot(place.along, z, place.core)
        if index % 2 == 1:
            send(source, place.along, z, place.x_next, len(sends))
        send(source, place.along, z, place.partner, len(sends))
    for step in order:
        z = place.z_peer(step)
        arrived(place.far, z, place.core)
        send(slot(place.far, z, place.core), place.far, z, place.partner, len(sends))
    for seq in (place.sp, place.across, place.along, place.far):
        for step in order:
            arrived(seq, place.z_peer(step), 1 - place.core)
    local.wait()
    for copy in sends:
        copy.wait_send()


def gather_rows(rows_in):
    rows, width = rows_in.shape
    depth = lax.axis_size("tp") // 2
    vmem = pl.BlockSpec(memory_space=pltpu.VMEM)
    count = depth - 1 + 3 * depth + 3 * depth + depth
    out = pl.pallas_call(
        gather_kernel,
        out_shape=jax.ShapeDtypeStruct((4, depth, 2, rows, width), rows_in.dtype),
        in_specs=[vmem],
        out_specs=vmem,
        scratch_shapes=[
            pltpu.SemaphoreType.DMA,
            pltpu.SemaphoreType.DMA((count,)),
            pltpu.SemaphoreType.DMA((4, depth, 2)),
        ],
        compiler_params=pltpu.CompilerParams(collective_id=1, has_side_effects=True),
    )(rows_in)
    return out.reshape(4 * depth * 2 * rows, width)


def add_into(target, first, *others):
    def one(z, nothing):
        total = first[z].astype(jnp.float32)
        for other in others:
            total = total + other[z].astype(jnp.float32)
        target[z] = total.astype(target.dtype)
        return nothing

    lax.fori_loop(0, target.shape[0], one, 0)


def finish_over_z(place, mine, z_recv, send_sems, recv_sems, base_ref, out_ref):
    copies = []
    order = [1] + list(range(place.depth - 1, 1, -1))
    for step in order:
        copy = remote(
            mine.at[place.z_peer(step)],
            z_recv.at[step - 1],
            send_sems.at[step - 1],
            recv_sems.at[step - 1],
            place.z_device(step),
        )
        copy.start()
        copies.append(copy)
    total = mine[place.z].astype(jnp.float32)
    for step, copy in zip(order, copies):
        copy.wait_recv()
        total = total + z_recv[step - 1].astype(jnp.float32)
    out_ref[...] = (base_ref[...].astype(jnp.float32) + total).astype(out_ref.dtype)
    for copy in copies:
        copy.wait_send()


def narrow_kernel(
    parts_ref, base_ref, out_ref, pair_recv, mine, z_recv, pair_send, pair_got, z_send, z_got
):
    place = Places()
    place.meet(False)
    copy = remote(
        parts_ref.at[1 - place.core], pair_recv, pair_send.at[0], pair_got.at[0], place.partner
    )
    copy.start()
    copy.wait_recv()
    add_into(mine, parts_ref.at[place.core], pair_recv)
    finish_over_z(place, mine, z_recv, z_send, z_got, base_ref, out_ref)
    copy.wait_send()


def wide_kernel(
    parts_ref,
    base_ref,
    out_ref,
    pair_recv,
    half_sum,
    x_recv,
    y_recv,
    x_last,
    y_last,
    mine,
    z_recv,
    pair_send,
    pair_got,
    xy_send,
    xy_got,
    z_send,
    z_got,
):
    place = Places()
    half = place.depth // 2
    front, back = pl.ds(0, half), pl.ds(half, place.depth - half)
    place.meet(True)
    order = (place.far, place.across, place.along, place.sp)
    pairs = []
    for count, seq in enumerate(order):
        copy = remote(
            parts_ref.at[1 - place.core, seq],
            pair_recv.at[count],
            pair_send.at[count],
            pair_got.at[count],
            place.partner,
        )
        copy.start()
        pairs.append(copy)
    sends = []

    def send(source, target, count, device):
        copy = remote(source, target, xy_send.at[count], xy_got.at[count], device)
        copy.start()
        sends.append(copy)
        return copy

    def pair_sum(count):
        pairs[count].wait_recv()
        add_into(half_sum.at[count], parts_ref.at[place.core, order[count]], pair_recv.at[count])

    pair_sum(0)
    far_x = send(half_sum.at[0, front], x_recv.at[1], 0, place.x_next)
    far_y = send(half_sum.at[0, back], y_recv.at[1], 1, place.y_next)
    pair_sum(1)
    near_x = send(half_sum.at[1, front], x_recv.at[0], 2, place.x_next)
    pair_sum(2)
    near_y = send(half_sum.at[2, back], y_recv.at[0], 3, place.y_next)
    pair_sum(3)
    far_x.wait_recv()
    add_into(x_recv.at[1], half_sum.at[2, front], x_recv.at[1])
    last_y = send(x_recv.at[1], y_last, 4, place.y_next)
    far_y.wait_recv()
    add_into(y_recv.at[1], half_sum.at[1, back], y_recv.at[1])
    last_x = send(y_recv.at[1], x_last, 5, place.x_next)
    near_x.wait_recv()
    near_y.wait_recv()
    last_y.wait_recv()
    add_into(mine.at[front], half_sum.at[3, front], x_recv.at[0], y_last)
    last_x.wait_recv()
    add_into(mine.at[back], half_sum.at[3, back], y_recv.at[0], x_last)
    finish_over_z(place, mine, z_recv, z_send, z_got, base_ref, out_ref)
    for copy in pairs + sends:
        copy.wait_send()


def scatter_sum(parts, base, out_dtype):
    rows, width = base.shape
    depth = lax.axis_size("tp") // 2
    vmem = pl.BlockSpec(memory_space=pltpu.VMEM)
    wide = parts.shape[0] > depth * 2 * rows
    half = depth // 2

    def room(*lead):
        return pltpu.VMEM(lead + (rows, width), jnp.bfloat16)

    def sems(count):
        return pltpu.SemaphoreType.DMA((count,))

    ends = [room(depth), room(depth - 1)]
    tail = [sems(depth - 1), sems(depth - 1)]
    if wide:
        shaped = parts.reshape(4, depth, 2, rows, width).transpose(2, 0, 1, 3, 4)
        body = wide_kernel
        scratch = [room(4, depth), room(4, depth), room(2, half), room(2, depth - half)]
        scratch = scratch + [room(depth - half), room(half)] + ends
        scratch = scratch + [sems(4), sems(4), sems(6), sems(6)] + tail
    else:
        shaped = parts.reshape(depth, 2, rows, width).transpose(1, 0, 2, 3)
        body = narrow_kernel
        scratch = [room(depth)] + ends + [sems(1), sems(1)] + tail
    return pl.pallas_call(
        body,
        out_shape=jax.ShapeDtypeStruct((rows, width), out_dtype),
        in_specs=[vmem] * 2,
        out_specs=vmem,
        scratch_shapes=scratch,
        compiler_params=pltpu.CompilerParams(
            collective_id=2 if wide else 0, has_side_effects=True, vmem_limit_bytes=60 * 2**20
        ),
    )(shaped, base)


def on_device(
    queries,
    keys,
    values,
    key_bias,
    head_gain,
    out_weight,
    residual,
    norm_gain,
    gate_proj,
    up_proj,
    down_proj,
    expert_choice,
    expert_weights,
):
    rows_own = queries.shape[0]
    model_width = out_weight.shape[1]
    seq_devices = lax.axis_size("sp")
    head_devices = lax.axis_size("tp")
    row_share = rows_own // head_devices
    local_experts = gate_proj.shape[0]
    experts_all = local_experts * seq_devices
    capacity = 4 * rows_own // (head_devices * experts_all)
    dense = capacity >= row_share and seq_devices == 4 and head_devices % 4 == 0
    if dense:
        named = expert_choice[:, :, None] == jnp.arange(experts_all, dtype=jnp.int32)
        own_weights = jnp.sum(jnp.where(named, expert_weights[:, :, None], 0.0), axis=1)
        all_weights = lax.all_gather(own_weights, ("sp", "tp"), axis=0, tiled=True)
        queries, all_weights = lax.optimization_barrier((queries, all_weights))
    attended = attention(queries, keys, values, key_bias, head_gain)
    shares = jnp.dot(attended, out_weight, preferred_element_type=jnp.float32)
    stream = scatter_sum(shares.astype(jnp.bfloat16), residual, jnp.bfloat16)
    normed = (rms_scaled(stream.astype(jnp.float32)) * norm_gain).astype(jnp.bfloat16)
    if dense:
        all_rows = gather_rows(normed)
        total = 0.0
        for local in range(local_experts):
            expert = lax.axis_index("sp") * local_experts + local
            weight = lax.dynamic_slice_in_dim(all_weights, expert, 1, 1)
            share = expert_partial(all_rows, gate_proj[local], up_proj[local], down_proj[local])
            total = total + jnp.where(weight > 0.0, weight * share, 0.0)
        return scatter_sum(total.astype(jnp.bfloat16), stream, jnp.bfloat16)
    own_slots = expert_choice * capacity + choice_ranks(expert_choice, experts_all)
    wanted = slot_tokens(own_slots, experts_all * capacity, row_share)
    outgoing = jnp.take(normed, wanted, axis=0, mode="fill", fill_value=0)
    arrived = lax.all_to_all(
        outgoing.reshape(seq_devices, local_experts, capacity, model_width),
        "sp",
        split_axis=0,
        concat_axis=0,
        tiled=True,
    )
    row_piece = lax.all_gather(arrived, "tp", axis=0, tiled=True)
    count_rows = row_piece.shape[0]
    partials = jnp.stack(
        [
            expert_partial(
                row_piece[:, 0].reshape(-1, model_width), gate_proj[0], up_proj[0], down_proj[0]
            ).reshape(count_rows, capacity, model_width)
        ],
        axis=1,
    )
    summed = lax.psum_scatter(partials.astype(jnp.bfloat16), "tp", scatter_dimension=0, tiled=True)
    returned = lax.all_to_all(summed, "sp", split_axis=0, concat_axis=0, tiled=True).reshape(
        experts_all * capacity, model_width
    )
    picked = jnp.take(returned, own_slots, axis=0).astype(jnp.float32)
    combined = jnp.sum(expert_weights[:, :, None] * picked, axis=1)
    return (stream.astype(jnp.float32) + combined).astype(jnp.bfloat16)


def solution(mesh):
    placed = (
        P("sp", "tp"),
        P("sp", "tp"),
        P("sp", "tp"),
        P("sp", "tp"),
        P("tp", None),
        P("tp", None),
        P(("sp", "tp"), None),
        P(),
        P("sp", None, "tp"),
        P("sp", None, "tp"),
        P("sp", "tp", None),
        P(("sp", "tp"), None),
        P(("sp", "tp"), None),
    )
    return jax.shard_map(
        on_device, mesh=mesh, in_specs=placed, out_specs=P(("sp", "tp"), None), check_vma=False
    )
```

profile of v0, /device:TPU:0, one launch (start us, length us, event | category | flops | bytes accessed | tf_op | source)
XLA Modules:
  0.0 253.4 jit_solution(2966264476389115976)
XLA Ops:
  6.5 0.0 copy-start
  6.5 0.8 reshape.35
  7.4 1.8 pad_maximum_fusion
  9.2 0.0 all-gather.4.cloned.1.call-update
  9.2 1.4 reshape.38.gain_ref
  10.6 0.7 select_reduce_fusion
  11.3 43.7 %all-gather.1 = f32[32,48,4]{1,2,0:T(4,128)S(1)} all-gather(f32[1,48,4]{1,2,0:T(4,128)S(1)} %bitcast.41), channel_id=1, replica_groups=mesh['sp'=4,'tp'=8] {'sp','tp'}, dimensions={0}, use_global_device_ids=true | all-gather | bytes 25344 | tf_op jit(solution)/shard_map/all_gather | solution.py:498
  55.0 0.1 reshape.45
  55.2 1.3 bitcast_convert_fusion.bias_ref
  56.4 6.9 %shard_map.127 = (f32[384,256]{1,0:T(8,128)}, f32[384,256]{1,0:T(8,128)}) custom-call(bf16[384,256]{1,0:T(8,128)(2,1)} %query_ref.1, bf16[384,256]{1,0:T(8,128)(2,1)} %key_ref.1, bf16[384,256]{1,0:T(8,128)(2,1)} %value_ref.1, f32[4,384]{1,0:T(4,128)} %bitcast_convert_fusion.bias_ref), custom_call_target="tpu_custom_call" | custom-call | flops 1179648000 | bytes 1000000 | tf_op jit(solution)/shard_map/pallas_call | solution.py:167
  63.4 0.8 slice_bitcast_fusion
  64.2 0.6 reshape.42.bias_ref
  64.8 2.9 %shard_map.128 = bf16[384,256]{1,0:T(8,128)(2,1)} custom-call(bf16[384,256]{1,0:T(8,128)(2,1)} %query_ref.1, bf16[4,392,512]{2,1,0:T(8,128)(2,1)} %bitcast.43, f32[4,4,384]{2,1,0:T(4,128)} %reshape.42.bias_ref, f32[384,256]{1,0:T(8,128)} %get-tuple-element.11.mix_in, f32[384,256]{1,0:T(8,128)} %get-tuple-element.12.carry_in, f32[1,256]{1,0:T(1,128)} %reshape.38.gain_ref), custom_call_target="tpu_custom_call" | custom-call | flops 2359296000 | bytes 1000000 | tf_op jit(solution)/shard_map/pallas_call | solution.py:176
  67.6 1.5 convolution_convert_fusion
  69.2 1.3 copy.36
  70.4 25.3 %shard_map.129.base_ref = bf16[48,2048]{1,0:T(8,128)(2,1)} custom-call(bf16[2,4,48,2048]{3,2,1,0:T(8,128)(2,1)} %bitcast.38, bf16[48,2048]{1,0:T(8,128)(2,1)} %base_ref.1), custom_call_target="tpu_custom_call" | custom-call | tf_op jit(solution)/shard_map/pallas_call | solution.py:459
  95.8 1.1 fusion.7
  96.9 1.7 fusion.9.own_ref
  98.6 50.8 %shard_map.130 = bf16[4,4,2,48,2048]{4,3,2,1,0:T(8,128)(2,1)} custom-call(bf16[48,2048]{1,0:T(8,128)(2,1)} %fusion.9.own_ref), custom_call_target="tpu_custom_call" | custom-call | tf_op jit(solution)/shard_map/pallas_call | solution.py:299
  149.4 11.3 %fusion.4 = f32[1536,896]{1,0:T(8,128)} fusion(bf16[1536,2048]{1,0:T(8,128)(2,1)} %bitcast.34, bf16[1,2048,896]{2,1,0:T(8,128)(2,1)} %param.21), kind=kOutput, calls=%fused_computation.5 | convolution fusion | flops 5637144576 | bytes 15466496 | tf_op jit(solution)/shard_map/dot_general | solution.py:18
  160.8 20.3 %select_convert_fusion = bf16[1536,2048]{1,0:T(8,128)(2,1)} fusion(f32[1536]{0:T(1024)S(1)} %dynamic-slice_reduce_fusion, pred[1536]{0:T(1024)(128)(4,1)S(1)} %compare_reduce_fusion, bf16[1,896,2048]{2,1,0:T(8,128)(2,1)} %param.23, f32[1536,896]{1,0:T(8,128)} %fusion.4, bf16[1536,2048]{1,0:T(8,128)(2,1)} %bitcast.35, bf16[1,2048,896]{2,1,0:T(8,128)(2,1)} %param.22), kind=kOutput, calls=%fused_computation | convolution fusion | flops 11291983872 | bytes 25435648 | tf_op jit(solution)/shard_map/dot_general | solution.py:21
  181.1 6.6 %copy.35 = bf16[4,4,2,48,2048]{4,3,1,0,2:T(8,128)(2,1)} copy(bf16[4,4,2,48,2048]{4,3,2,1,0:T(8,128)(2,1)} %bitcast.36) | data formatting | bytes 12582912 | tf_op jit(solution)/shard_map/reshape | solution.py:450
  187.6 57.3 %shard_map.131 = bf16[48,2048]{1,0:T(8,128)(2,1)} custom-call(bf16[2,4,4,48,2048]{4,3,2,1,0:T(8,128)(2,1)} %bitcast.33, bf16[48,2048]{1,0:T(8,128)(2,1)} %shard_map.129.base_ref), custom_call_target="tpu_custom_call" | custom-call | tf_op jit(solution)/shard_map/pallas_call | solution.py:459
  245.0 1.6 copy.38
  (13 shorter events, 0.1 us)
Async XLA Ops:
  6.5 61.1 %copy-start = (bf16[256,2048]{1,0:T(8,128)(2,1)S(1)}, bf16[256,2048]{1,0:T(8,128)(2,1)}, u32[]{:S(2)}) copy-start(bf16[256,2048]{1,0:T(8,128)(2,1)} %param.18) | copy-start | bytes 3145732
  6.5 56.8 %all-gather.4.cloned.1.call-start = ((), (), s32[]{:S(2)}) async-start(), calls=%async_computation | async-start | bytes 2007040 | tf_op jit(solution)/shard_map/all_gather | solution.py:163
  67.6 29.2 %copy-start.1 = (f32[2048]{0:T(1024)S(1)}, f32[2048]{0:T(1024)}, u32[]{:S(2)}) copy-start(f32[2048]{0:T(1024)} %param.20) | copy-start | bytes 24580
Sparse Core Ops, SparseCore 0:
  9.3 33.9 all-gather.3
where the time goes:
time: 254 us; the launch traced here: 253 us
  Pallas kernels  143 us (56%)
  blocking collectives  43.7 us (17%)
  matrix products  33.2 us (13%)
  between operations  13.5 us (5%)
  local copies, waits for them, and re-layouts  13.2 us (5%)
  other arithmetic  6.65 us (3%)
    pallas_call x2, Pallas kernels, scatter_sum(): pl.pallas_call(body, out_shape=jax.ShapeDtypeStruct((rows, width), out_dt...  82.7 us
    pallas_call x1, Pallas kernels, gather_rows(): pl.pallas_call(gather_kernel, out_shape=jax.ShapeDtypeStruct((4, depth, 2...  50.8 us
    all_gather x1, blocking collectives, on_device(): all_weights = lax.all_gather(own_weights, ('sp', 'tp'), axis=0, tiled=True)  43.7 us
    dot_general x1, matrix products, expert_partial(): return jnp.dot(hidden, down_matrix, preferred_element_type=jnp.float32)  20.3 us
    dot_general x1, matrix products, expert_partial(): jnp.dot(row_block, gate_matrix, preferred_element_type=jnp.float32)  11.3 us
    pallas_call x1, Pallas kernels, attention(): pl.pallas_call(functools.partial(diagonal_kernel, head_size), out_shape=[...  6.91 us
    reshape x1, local copies, waits for them, and re-layouts, scatter_sum(): shaped = parts.reshape(4, depth, 2, rows, width).transpose(2, 0, 1, 3, 4)  6.56 us
  transfers between devices with their start and end apart: 1, of which 0 were waited for; matrix products, arithmetic and copies ran while one was open for 1% of the time, Pallas kernels for 3%

commit v1 on v0

--- a/solution.py
+++ b/solution.py
@@ -228,89 +228,6 @@
     )
 
 
-def gather_kernel(own_ref, out_ref, local_sem, send_sems, recv_sems):
-    place = Places()
-    depth = place.depth
-    place.meet(True)
-    sends = []
-
-    def slot(seq, z, core):
-        return out_ref.at[seq, z, core]
-
-    def send(source, seq, z, device, count):
-        copy = remote(
-            source,
-            slot(seq, z, place.core),
-            send_sems.at[count],
-            recv_sems.at[seq, z, place.core],
-            device,
-        )
-        copy.start()
-        sends.append(copy)
-
-    def arrived(seq, z, core):
-        remote(
-            own_ref, slot(seq, z, core), send_sems.at[0], recv_sems.at[seq, z, core], place.partner
-        ).wait_recv()
-
-    local = pltpu.make_async_copy(own_ref, slot(place.sp, place.z, place.core), local_sem)
-    local.start()
-    order = [0, 1] + list(range(depth - 1, 1, -1))
-    for step in order[1:]:
-        send(own_ref, place.sp, place.z, place.z_device(step), len(sends))
-    for step in order:
-        z = place.z_peer(step)
-        source = own_ref
-        if step > 0:
-            arrived(place.sp, z, place.core)
-            source = slot(place.sp, z, place.core)
-        send(source, place.sp, z, place.x_next, len(sends))
-        send(source, place.sp, z, place.y_next, len(sends))
-        send(source, place.sp, z, place.partner, len(sends))
-    for index, step in enumerate(order):
-        z = place.z_peer(step)
-        arrived(place.across, z, place.core)
-        source = slot(place.across, z, place.core)
-        if index % 2 == 0:
-            send(source, place.across, z, place.y_next, len(sends))
-        send(source, place.across, z, place.partner, len(sends))
-        arrived(place.along, z, place.core)
-        source = slot(place.along, z, place.core)
-        if index % 2 == 1:
-            send(source, place.along, z, place.x_next, len(sends))
-        send(source, place.along, z, place.partner, len(sends))
-    for step in order:
-        z = place.z_peer(step)
-        arrived(place.far, z, place.core)
-        send(slot(place.far, z, place.core), place.far, z, place.partner, len(sends))
-    for seq in (place.sp, place.across, place.along, place.far):
-        for step in order:
-            arrived(seq, place.z_peer(step), 1 - place.core)
-    local.wait()
-    for copy in sends:
-        copy.wait_send()
-
-
-def gather_rows(rows_in):
-    rows, width = rows_in.shape
-    depth = lax.axis_size("tp") // 2
-    vmem = pl.BlockSpec(memory_space=pltpu.VMEM)
-    count = depth - 1 + 3 * depth + 3 * depth + depth
-    out = pl.pallas_call(
-        gather_kernel,
-        out_shape=jax.ShapeDtypeStruct((4, depth, 2, rows, width), rows_in.dtype),
-        in_specs=[vmem],
-        out_specs=vmem,
-        scratch_shapes=[
-            pltpu.SemaphoreType.DMA,
-            pltpu.SemaphoreType.DMA((count,)),
-            pltpu.SemaphoreType.DMA((4, depth, 2)),
-        ],
-        compiler_params=pltpu.CompilerParams(collective_id=1, has_side_effects=True),
-    )(rows_in)
-    return out.reshape(4 * depth * 2 * rows, width)
-
-
 def add_into(target, first, *others):
     def one(z, nothing):
         total = first[z].astype(jnp.float32)
@@ -359,84 +276,10 @@
     copy.wait_send()
 
 
-def wide_kernel(
-    parts_ref,
-    base_ref,
-    out_ref,
-    pair_recv,
-    half_sum,
-    x_recv,
-    y_recv,
-    x_last,
-    y_last,
-    mine,
-    z_recv,
-    pair_send,
-    pair_got,
-    xy_send,
-    xy_got,
-    z_send,
-    z_got,
-):
-    place = Places()
-    half = place.depth // 2
-    front, back = pl.ds(0, half), pl.ds(half, place.depth - half)
-    place.meet(True)
-    order = (place.far, place.across, place.along, place.sp)
-    pairs = []
-    for count, seq in enumerate(order):
-        copy = remote(
-            parts_ref.at[1 - place.core, seq],
-            pair_recv.at[count],
-            pair_send.at[count],
-            pair_got.at[count],
-            place.partner,
-        )
-        copy.start()
-        pairs.append(copy)
-    sends = []
-
-    def send(source, target, count, device):
-        copy = remote(source, target, xy_send.at[count], xy_got.at[count], device)
-        copy.start()
-        sends.append(copy)
-        return copy
-
-    def pair_sum(count):
-        pairs[count].wait_recv()
-        add_into(half_sum.at[count], parts_ref.at[place.core, order[count]], pair_recv.at[count])
-
-    pair_sum(0)
-    far_x = send(half_sum.at[0, front], x_recv.at[1], 0, place.x_next)
-    far_y = send(half_sum.at[0, back], y_recv.at[1], 1, place.y_next)
-    pair_sum(1)
-    near_x = send(half_sum.at[1, front], x_recv.at[0], 2, place.x_next)
-    pair_sum(2)
-    near_y = send(half_sum.at[2, back], y_recv.at[0], 3, place.y_next)
-    pair_sum(3)
-    far_x.wait_recv()
-    add_into(x_recv.at[1], half_sum.at[2, front], x_recv.at[1])
-    last_y = send(x_recv.at[1], y_last, 4, place.y_next)
-    far_y.wait_recv()
-    add_into(y_recv.at[1], half_sum.at[1, back], y_recv.at[1])
-    last_x = send(y_recv.at[1], x_last, 5, place.x_next)
-    near_x.wait_recv()
-    near_y.wait_recv()
-    last_y.wait_recv()
-    add_into(mine.at[front], half_sum.at[3, front], x_recv.at[0], y_last)
-    last_x.wait_recv()
-    add_into(mine.at[back], half_sum.at[3, back], y_recv.at[0], x_last)
-    finish_over_z(place, mine, z_recv, z_send, z_got, base_ref, out_ref)
-    for copy in pairs + sends:
-        copy.wait_send()
-
-
 def scatter_sum(parts, base, out_dtype):
     rows, width = base.shape
     depth = lax.axis_size("tp") // 2
     vmem = pl.BlockSpec(memory_space=pltpu.VMEM)
-    wide = parts.shape[0] > depth * 2 * rows
-    half = depth // 2
 
     def room(*lead):
         return pltpu.VMEM(lead + (rows, width), jnp.bfloat16)
@@ -444,28 +287,335 @@
     def sems(count):
         return pltpu.SemaphoreType.DMA((count,))
 
-    ends = [room(depth), room(depth - 1)]
-    tail = [sems(depth - 1), sems(depth - 1)]
-    if wide:
-        shaped = parts.reshape(4, depth, 2, rows, width).transpose(2, 0, 1, 3, 4)
-        body = wide_kernel
-        scratch = [room(4, depth), room(4, depth), room(2, half), room(2, depth - half)]
-        scratch = scratch + [room(depth - half), room(half)] + ends
-        scratch = scratch + [sems(4), sems(4), sems(6), sems(6)] + tail
-    else:
-        shaped = parts.reshape(depth, 2, rows, width).transpose(1, 0, 2, 3)
-        body = narrow_kernel
-        scratch = [room(depth)] + ends + [sems(1), sems(1)] + tail
+    shaped = parts.reshape(depth, 2, rows, width).transpose(1, 0, 2, 3)
     return pl.pallas_call(
-        body,
+        narrow_kernel,
         out_shape=jax.ShapeDtypeStruct((rows, width), out_dtype),
         in_specs=[vmem] * 2,
         out_specs=vmem,
-        scratch_shapes=scratch,
+        scratch_shapes=[room(depth), room(depth), room(depth - 1)]
+        + [sems(1), sems(1), sems(depth - 1), sems(depth - 1)],
         compiler_params=pltpu.CompilerParams(
-            collective_id=2 if wide else 0, has_side_effects=True, vmem_limit_bytes=60 * 2**20
+            collective_id=0, has_side_effects=True, vmem_limit_bytes=60 * 2**20
         ),
     )(shaped, base)
+
+
+class Sends:
+    def __init__(self, sems):
+        self.sems = sems
+        self.made = []
+
+    def start(self, source, target, recv_sem, device, when=None):
+        copy = remote(source, target, self.sems.at[len(self.made)], recv_sem, device)
+        self.made.append((copy, when))
+        if when is None:
+            copy.start()
+        else:
+            pl.when(when)(copy.start)
+
+    def finish(self):
+        for copy, when in self.made:
+            if when is None:
+                copy.wait_send()
+            else:
+                pl.when(when)(copy.wait_send)
+
+
+def plane_order(z, depth, step):
+    near = jnp.minimum(z, depth - 1 - z)
+    if step % 2 == 1:
+        swing = z - (step + 1) // 2
+    else:
+        swing = z + step // 2
+    rest = jnp.where(z == near, step, depth - 1 - step)
+    return jnp.where(step <= 2 * near, swing, rest)
+
+
+def layer_kernel(
+    own_ref,
+    stream_ref,
+    gate_ref,
+    up_ref,
+    down_ref,
+    out_ref,
+    rows_buf,
+    pair_w,
+    down_w,
+    hidden,
+    parts,
+    pair_recv,
+    x_far,
+    y_far,
+    x_near,
+    y_near,
+    x_last,
+    y_last,
+    totals,
+    z_recv,
+    local_sem,
+    weight_sems,
+    send_sems,
+    z_got,
+    x_got,
+    y_got,
+    far_got,
+    side_got,
+    pair_got,
+    cross_got,
+    z_sum_got,
+):
+    place = Places()
+    depth, core, own_z = place.depth, place.core, place.z
+    rows, width = out_ref.shape
+    wide = own_ref.shape[1]
+    count = 8 * rows
+    half = width // 2
+    cut = wide // 256 * 128
+    hidden_width = hidden.shape[1]
+    tile = 128
+    copies = []
+    for index in range(hidden_width // tile):
+        for which, source in enumerate((gate_ref, up_ref)):
+            copies.append(
+                pltpu.make_async_copy(
+                    source.at[:, pl.ds(index * tile, tile)],
+                    pair_w.at[:, pl.ds((2 * index + which) * tile, tile)],
+                    weight_sems.at[len(copies)],
+                )
+            )
+    copies.append(pltpu.make_async_copy(down_ref, down_w, weight_sems.at[len(copies)]))
+    for copy in copies:
+        copy.start()
+    place.meet(True)
+    sends = Sends(send_sems)
+    planes = [plane_order(own_z, depth, step) for step in range(depth)]
+    front, back = pl.ds(0, cut), pl.ds(cut, wide - cut)
+    left, right = pl.ds(0, half), pl.ds(half, half)
+    z_up = (place.sp, (own_z + 1) * 2 + core)
+    z_down = (place.sp, (own_z - 1) * 2 + core)
+    has_up, has_down = own_z < depth - 1, own_z > 0
+
+    def slot(step, seq):
+        return rows_buf.at[planes[step], core, seq]
+
+    def wait_for(target, sem):
+        remote(target, target, send_sems.at[0], sem, place.partner).wait_recv()
+
+    def to_partner(step, seq, source=None):
+        target = slot(step, seq)
+        sends.start(
+            target if source is None else source,
+            target,
+            side_got.at[planes[step], seq],
+            place.partner,
+        )
+
+    def own(step):
+        plane = planes[step]
+        target = slot(step, place.sp)
+        source = own_ref
+        if step > 0:
+            wait_for(target, z_got.at[plane])
+            source = target
+            go_up = jnp.logical_and(has_up, plane < own_z)
+            go_down = jnp.logical_and(has_down, plane > own_z)
+        else:
+            go_up, go_down = has_up, has_down
+        if depth > 1:
+            sends.start(source, target, z_got.at[plane], z_up, go_up)
+            sends.start(source, target, z_got.at[plane], z_down, go_down)
+        sends.start(source, target, x_got.at[plane], place.x_next)
+        sends.start(source, target, y_got.at[plane], place.y_next)
+        to_partner(step, place.sp, source)
+
+    def relay(step):
+        plane = planes[step]
+        across, along = slot(step, place.across), slot(step, place.along)
+        wait_for(across, x_got.at[plane])
+        sends.start(across.at[:, front], across.at[:, front], far_got.at[plane, 0], place.y_next)
+        wait_for(along, y_got.at[plane])
+        sends.start(along.at[:, back], along.at[:, back], far_got.at[plane, 1], place.x_next)
+        to_partner(step, place.across)
+        to_partner(step, place.along)
+
+    def far(step):
+        plane = planes[step]
+        target = slot(step, place.far)
+        wait_for(target.at[:, front], far_got.at[plane, 0])
+        wait_for(target.at[:, back], far_got.at[plane, 1])
+        to_partner(step, place.far)
+
+    def ready(step):
+        plane = planes[step]
+        for seq in (place.sp, place.across, place.along, place.far):
+            wait_for(rows_buf.at[plane, 1 - core, seq], side_got.at[plane, seq])
+
+    def compute(step):
+        plane = planes[step]
+
+        def open_tile(index, nothing):
+            spot = pl.multiple_of(index * 2 * tile, 2 * tile)
+            block = rows_buf[plane, :, :, :, :width].reshape(count, width)
+            both = jnp.dot(
+                block, pair_w[:, pl.ds(spot, 2 * tile)], preferred_element_type=jnp.float32
+            )
+            gate_part, up_part = both[:, :tile], both[:, tile:]
+            value = gate_part / (1.0 + jnp.exp(-gate_part)) * up_part
+            hidden[:, pl.ds(pl.multiple_of(index * tile, tile), tile)] = value.astype(jnp.bfloat16)
+            return nothing
+
+        lax.fori_loop(0, hidden_width // tile, open_tile, 0)
+        lane = lax.broadcasted_iota(jnp.int32, (count, tile), 1)
+        extra = rows_buf[plane, :, :, :, width:].reshape(count, tile).astype(jnp.float32)
+        mine = jnp.logical_or(lane == place.sp, lane == place.sp + 4)
+        weight = jnp.sum(jnp.where(mine, extra, 0.0), axis=1, keepdims=True)
+
+        def down_tile(index, nothing):
+            spot = pl.ds(pl.multiple_of(index * 2 * tile, 2 * tile), 2 * tile)
+            share = jnp.dot(hidden[...], down_w[:, spot], preferred_element_type=jnp.float32)
+            share = jnp.where(weight > 0.0, weight * share, 0.0).astype(jnp.bfloat16)
+            parts[step, :, :, :, spot] = share.reshape(2, 4, rows, 2 * tile)
+            return nothing
+
+        lax.fori_loop(0, width // (2 * tile), down_tile, 0)
+        sends.start(
+            parts.at[step, 1 - core], pair_recv.at[step], pair_got.at[step], place.partner
+        )
+
+    def first_sum(step):
+        wait_for(pair_recv.at[step], pair_got.at[step])
+        add_into(parts.at[step, core], parts.at[step, core], pair_recv.at[step])
+        mine = parts.at[step, core]
+        got = cross_got.at[step]
+        sends.start(mine.at[place.far, :, left], x_far.at[step], got.at[0], place.x_next)
+        sends.start(mine.at[place.far, :, right], y_far.at[step], got.at[1], place.y_next)
+        sends.start(mine.at[place.across, :, left], x_near.at[step], got.at[2], place.x_next)
+        sends.start(mine.at[place.along, :, right], y_near.at[step], got.at[3], place.y_next)
+
+    def plus(target, *others):
+        total = target.astype(jnp.float32)
+        for other in others:
+            total = total + other.astype(jnp.float32)
+        return total
+
+    def second_sum(step):
+        got = cross_got.at[step]
+        wait_for(x_far.at[step], got.at[0])
+        x_far[step] = plus(x_far[step], parts[step, core, place.along, :, left]).astype(jnp.bfloat16)
+        sends.start(x_far.at[step], y_last.at[step], got.at[4], place.y_next)
+        wait_for(y_far.at[step], got.at[1])
+        y_far[step] = plus(y_far[step], parts[step, core, place.across, :, right]).astype(jnp.bfloat16)
+        sends.start(y_far.at[step], x_last.at[step], got.at[5], place.x_next)
+
+    def third_sum(step):
+        got = cross_got.at[step]
+        wait_for(x_near.at[step], got.at[2])
+        wait_for(y_last.at[step], got.at[4])
+        low = plus(parts[step, core, place.sp, :, left], x_near[step], y_last[step])
+        wait_for(y_near.at[step], got.at[3])
+        wait_for(x_last.at[step], got.at[5])
+        high = plus(parts[step, core, place.sp, :, right], y_near[step], x_last[step])
+        if step > 0:
+            totals[step, :, left] = low.astype(jnp.bfloat16)
+            totals[step, :, right] = high.astype(jnp.bfloat16)
+            sends.start(
+                totals.at[step],
+                z_recv.at[own_z],
+                z_sum_got.at[own_z],
+                (place.sp, planes[step] * 2 + core),
+            )
+        else:
+            for shift in range(1, depth):
+                other = place.z_peer(shift)
+                wait_for(z_recv.at[other], z_sum_got.at[other])
+                low = plus(low, z_recv[other, :, left])
+                high = plus(high, z_recv[other, :, right])
+            out_ref[:, left] = plus(low, stream_ref[:, left]).astype(jnp.bfloat16)
+            out_ref[:, right] = plus(high, stream_ref[:, right]).astype(jnp.bfloat16)
+
+    local = pltpu.make_async_copy(own_ref, slot(0, place.sp), local_sem)
+    local.start()
+    own(0)
+    own(1)
+    relay(0)
+    for step in range(2, depth):
+        own(step)
+        far(step - 2)
+        relay(step - 1)
+    for copy in copies:
+        copy.wait()
+    local.wait()
+    order = list(range(1, depth)) + [0]
+    for index, step in enumerate(order):
+        if index == 1:
+            relay(depth - 1)
+        if step == depth - 2:
+            far(depth - 2)
+        if step == depth - 1:
+            far(depth - 1)
+        ready(step)
+        compute(step)
+        if index >= 1:
+            second_sum(order[index - 1])
+        if index >= 2:
+            third_sum(order[index - 2])
+        first_sum(step)
+    second_sum(order[-1])
+    third_sum(order[-2])
+    third_sum(order[-1])
+    sends.finish()
+
+
+def expert_layer(own_rows, stream, gate_matrix, up_matrix, down_matrix):
+    rows, width = stream.shape
+    wide = own_rows.shape[1]
+    depth = lax.axis_size("tp") // 2
+    hidden_width = gate_matrix.shape[1]
+    vmem = pl.BlockSpec(memory_space=pltpu.VMEM)
+    anywhere = pl.BlockSpec(memory_space=pl.ANY)
+
+    def room(*shape):
+        return pltpu.VMEM(shape, jnp.bfloat16)
+
+    def sems(*shape):
+        return pltpu.SemaphoreType.DMA(shape)
+
+    half = [room(depth, rows, width // 2)] * 6
+    total_sends = depth * (5 + 4 + 1 + 1 + 4 + 2) + depth - 1
+    return pl.pallas_call(
+        layer_kernel,
+        out_shape=jax.ShapeDtypeStruct((rows, width), jnp.bfloat16),
+        in_specs=[vmem, vmem, anywhere, anywhere, anywhere],
+        out_specs=vmem,
+        scratch_shapes=[
+            room(depth, 2, 4, rows, wide),
+            room(width, 2 * hidden_width),
+            room(hidden_width, width),
+            room(8 * rows, hidden_width),
+            room(depth, 2, 4, rows, width),
+            room(depth, 4, rows, width),
+        ]
+        + half
+        + [
+            room(depth, rows, width),
+            room(depth, rows, width),
+            pltpu.SemaphoreType.DMA,
+            sems(2 * (hidden_width // 128) + 1),
+            sems(total_sends),
+            sems(depth),
+            sems(depth),
+            sems(depth),
+            sems(depth, 2),
+            sems(depth, 4),
+            sems(depth),
+            sems(depth, 6),
+            sems(depth),
+        ],
+        compiler_params=pltpu.CompilerParams(
+            collective_id=1, has_side_effects=True, vmem_limit_bytes=60 * 2**20
+        ),
+    )(own_rows, stream, gate_matrix, up_matrix, down_matrix)
 
 
 def on_device(
@@ -492,24 +642,20 @@
     experts_all = local_experts * seq_devices
     capacity = 4 * rows_own // (head_devices * experts_all)
     dense = capacity >= row_share and seq_devices == 4 and head_devices % 4 == 0
+    dense = dense and local_experts == 1 and head_devices >= 8
     if dense:
         named = expert_choice[:, :, None] == jnp.arange(experts_all, dtype=jnp.int32)
         own_weights = jnp.sum(jnp.where(named, expert_weights[:, :, None], 0.0), axis=1)
-        all_weights = lax.all_gather(own_weights, ("sp", "tp"), axis=0, tiled=True)
-        queries, all_weights = lax.optimization_barrier((queries, all_weights))
     attended = attention(queries, keys, values, key_bias, head_gain)
     shares = jnp.dot(attended, out_weight, preferred_element_type=jnp.float32)
     stream = scatter_sum(shares.astype(jnp.bfloat16), residual, jnp.bfloat16)
     normed = (rms_scaled(stream.astype(jnp.float32)) * norm_gain).astype(jnp.bfloat16)
     if dense:
-        all_rows = gather_rows(normed)
-        total = 0.0
-        for local in range(local_experts):
-            expert = lax.axis_index("sp") * local_experts + local
-            weight = lax.dynamic_slice_in_dim(all_weights, expert, 1, 1)
-            share = expert_partial(all_rows, gate_proj[local], up_proj[local], down_proj[local])
-            total = total + jnp.where(weight > 0.0, weight * share, 0.0)
-        return scatter_sum(total.astype(jnp.bfloat16), stream, jnp.bfloat16)
+        high = lax.reduce_precision(own_weights, 8, 7)
+        blank = jnp.zeros((row_share, 128 - 2 * experts_all), jnp.bfloat16)
+        extra = [high.astype(jnp.bfloat16), (own_weights - high).astype(jnp.bfloat16), blank]
+        own_rows = jnp.concatenate([normed] + extra, axis=1)
+        return expert_layer(own_rows, stream, gate_proj[0], up_proj[0], down_proj[0])
     own_slots = expert_choice * capacity + choice_ranks(expert_choice, experts_all)
     wanted = slot_tokens(own_slots, experts_all * capacity, row_share)
     outgoing = jnp.take(normed, wanted, axis=0, mode="fill", fill_value=0)

time: 254 us -> 190 us (0.75)
  blocking collectives: 43.7 us -> 0 us
  matrix products: 33.2 us -> 1.5 us
  waiting for transfers between devices: 0.02 us -> 23.5 us
  Pallas kernels: 143 us -> 137 us
  local copies, waits for them, and re-layouts: 13.2 us -> 7.47 us
    all_gather x1 -> x0, blocking collectives: 43.7 us -> none  [on_device(): all_weights = lax.all_gather(own_weights, ('sp', 'tp'), axis=0, tiled=True)]
    dot_general x2 -> x0, matrix products: 31.6 us -> none  [the longest x1 20.3 us: expert_partial(): return jnp.dot(hidden, down_matrix, preferred_element_type=jnp.float32)]
    all_gather x1, waiting for transfers between devices: 0.01 us -> 23.5 us  [attention(): gathered = lax.all_gather(packed, 'sp', axis=0)]
    reshape x1 -> x0, local copies, waits for them, and re-layouts: 6.56 us -> none  [scatter_sum(): shaped = parts.reshape(4, depth, 2, rows, width).transpose(2, 0, 1, 3, 4)]
    pallas_call x3 -> x2, Pallas kernels: 133 us -> 128 us  [the longest x1 102 us: expert_layer(): pl.pallas_call(layer_kernel, out_shape=jax.ShapeDtypeStruct((rows, width)...]
  transfers between devices with their start and end apart: 1 -> 1, of which waited for: 0 -> 1; matrix products, arithmetic and copies ran while one was open for 1% -> 2% of each run, Pallas kernels for 3% -> 4%
where the time goes in v1:
time: 190 us; the launch traced here: 189 us
  Pallas kernels  137 us (72%)
  waiting for transfers between devices  23.5 us (12%)
  between operations  13.5 us (7%)
  local copies, waits for them, and re-layouts  7.47 us (4%)
  other arithmetic  5.93 us (3%)
    pallas_call x1, Pallas kernels, expert_layer(): pl.pallas_call(layer_kernel, out_shape=jax.ShapeDtypeStruct((rows, width)...  102 us
    pallas_call x1, Pallas kernels, scatter_sum(): pl.pallas_call(narrow_kernel, out_shape=jax.ShapeDtypeStruct((rows, width...  25.5 us
    all_gather x1, waiting for transfers between devices, attention(): gathered = lax.all_gather(packed, 'sp', axis=0)  23.5 us
    pallas_call x1, Pallas kernels, attention(): pl.pallas_call(functools.partial(diagonal_kernel, head_size), out_shape=[...  6.93 us
  transfers between devices with their start and end apart: 1, of which 1 were waited for; matrix products, arithmetic and copies ran while one was open for 2% of the time, Pallas kernels for 4%

profile of v1, /device:TPU:0, one launch (start us, length us, event | category | flops | bytes accessed | tf_op | source)
XLA Modules:
  0.0 189.2 jit_solution(9448616430819804718)
XLA Ops:
  6.5 0.0 copy-start
  6.5 0.0 all-gather.3.cloned.1.call-start
  6.5 0.8 reshape.29
  7.4 1.8 pad_maximum_fusion
  9.2 0.0 all-gather.3.cloned.1.call-update
  9.2 1.3 reshape.32.gain_ref
  10.5 0.7 select_reduce_fusion
  11.2 0.1 copy.23
  11.3 0.1 copy.24
  11.4 0.1 copy.25
  11.5 1.3 bitcast_convert_fusion.bias_ref
  12.8 6.9 %shard_map.127 = (f32[384,256]{1,0:T(8,128)}, f32[384,256]{1,0:T(8,128)}) custom-call(bf16[384,256]{1,0:T(8,128)(2,1)} %query_ref.3, bf16[384,256]{1,0:T(8,128)(2,1)} %key_ref.1, bf16[384,256]{1,0:T(8,128)(2,1)} %value_ref.1, f32[4,384]{1,0:T(4,128)} %bitcast_convert_fusion.bias_ref), custom_call_target="tpu_custom_call" | custom-call | flops 1179648000 | bytes 1000000 | tf_op jit(solution)/shard_map/pallas_call | solution.py:167
  19.7 23.5 %all-gather.3.cloned.1.call-done = bf16[1568,512]{1,0:T(8,128)(2,1)} async-done(((bf16[392,512]{1,0:T(8,128)(2,1)}), bf16[1568,512]{1,0:T(8,128)(2,1)}) %all-gather.3.cloned.1.call-update) | async-done | bytes 1605648 | tf_op jit(solution)/shard_map/all_gather | solution.py:163
  43.2 0.8 slice_bitcast_fusion
  44.0 0.6 reshape.34.bias_ref
  44.6 2.9 %shard_map.128 = bf16[384,256]{1,0:T(8,128)(2,1)} custom-call(bf16[384,256]{1,0:T(8,128)(2,1)} %query_ref.3, bf16[4,392,512]{2,1,0:T(8,128)(2,1)} %bitcast.23, f32[4,4,384]{2,1,0:T(4,128)} %reshape.34.bias_ref, f32[384,256]{1,0:T(8,128)} %get-tuple-element.7.mix_in, f32[384,256]{1,0:T(8,128)} %get-tuple-element.8.carry_in, f32[1,256]{1,0:T(1,128)} %reshape.32.gain_ref), custom_call_target="tpu_custom_call" | custom-call | flops 2359296000 | bytes 1000000 | tf_op jit(solution)/shard_map/pallas_call | solution.py:176
  47.5 1.5 convolution_convert_fusion
  49.0 1.3 copy.28
  50.2 25.5 %shard_map.129.stream_ref = bf16[48,2048]{1,0:T(8,128)(2,1)} custom-call(bf16[2,4,48,2048]{3,2,1,0:T(8,128)(2,1)} %bitcast.16, bf16[48,2048]{1,0:T(8,128)(2,1)} %base_ref.1), custom_call_target="tpu_custom_call" | custom-call | tf_op jit(solution)/shard_map/pallas_call | solution.py:291
  75.7 1.1 fusion
  76.8 1.0 fusion.2
  77.9 0.8 concatenate.11.own_ref
  78.6 102.1 %shard_map.130 = bf16[48,2048]{1,0:T(8,128)(2,1)} custom-call(bf16[48,2176]{1,0:T(8,128)(2,1)} %concatenate.11.own_ref, bf16[48,2048]{1,0:T(8,128)(2,1)} %shard_map.129.stream_ref, bf16[2048,896]{1,0:T(8,128)(2,1)} %bitcast.17, bf16[2048,896]{1,0:T(8,128)(2,1)} %bitcast.18, bf16[896,2048]{1,0:T(8,128)(2,1)} %bitcast.19), custom_call_target="tpu_custom_call" | custom-call | tf_op jit(solution)/shard_map/pallas_call | solution.py:586
  180.7 1.6 copy.30
  (11 shorter events, 0.1 us)
Async XLA Ops:
  6.5 40.9 %copy-start = (bf16[256,2048]{1,0:T(8,128)(2,1)S(1)}, bf16[256,2048]{1,0:T(8,128)(2,1)}, u32[]{:S(2)}) copy-start(bf16[256,2048]{1,0:T(8,128)(2,1)} %param.18) | copy-start | bytes 3145732
  6.5 36.6 %all-gather.3.cloned.1.call-start = ((), (), s32[]{:S(2)}) async-start(), calls=%async_computation | async-start | bytes 2007040 | tf_op jit(solution)/shard_map/all_gather | solution.py:163
  50.2 26.6 %copy-start.1 = (f32[2048]{0:T(1024)S(1)}, f32[2048]{0:T(1024)}, u32[]{:S(2)}) copy-start(f32[2048]{0:T(1024)} %param.20) | copy-start | bytes 24580
Sparse Core Ops, SparseCore 0:
  9.3 33.8 all-gather.2

commit v2 on v1

--- a/solution.py
+++ b/solution.py
@@ -1,4 +1,5 @@
 import functools
+import types
 
 import jax
 import jax.numpy as jnp
@@ -39,6 +40,45 @@
 def softplus_parts(scores):
     drops = -jnp.maximum(scores, 0.0) - jnp.log(1.0 + jnp.exp(-jnp.abs(scores)))
     return drops, scores + drops
+
+
+def block_weights(query, key_tile, bias_row, mine, later, diagonal):
+    rows = query.shape[0]
+    query = jnp.where(mine, query, jnp.zeros_like(query))
+    scores = lax.dot_general(
+        query, key_tile, (((1,), (1,)), ((), ())), preferred_element_type=jnp.float32
+    )
+    scores = scores + bias_row
+    drops, hits = softplus_parts(scores)
+    if diagonal:
+        row_pos = lax.broadcasted_iota(jnp.int32, (rows, rows), 0)
+        col_pos = lax.broadcasted_iota(jnp.int32, (rows, rows), 1)
+        earlier = col_pos < row_pos
+        drops = jnp.where(earlier, drops, 0.0)
+    suffix = jnp.dot(drops.astype(jnp.bfloat16), later, preferred_element_type=jnp.float32)
+    within = jnp.exp(hits + suffix)
+    if diagonal:
+        within = jnp.where(earlier, within, 0.0)
+    return within.astype(jnp.bfloat16), suffix[:, 0:1] + drops[:, 0:1]
+
+
+def attend(query_ref, key_of, value_of, bias_of, later_ref, part_ref, total_ref, head_size, diagonal, group):
+    lanes = 128
+    per_group = lanes // head_size
+    lane_head = lax.broadcasted_iota(jnp.int32, (1, lanes), 1) // head_size
+    cols = slice(group * lanes, (group + 1) * lanes)
+    query = query_ref[:, cols] * jnp.asarray(head_size**-0.5, jnp.bfloat16)
+    part_all, total_all = 0.0, 0.0
+    for inner in range(per_group):
+        mine = lane_head == inner
+        weights, total = block_weights(
+            query, key_of(cols), bias_of(group * per_group + inner), mine, later_ref[...], diagonal
+        )
+        part = jnp.dot(weights, value_of(cols), preferred_element_type=jnp.float32)
+        part_all = jnp.where(mine, part, part_all)
+        total_all = jnp.where(mine, total, total_all)
+    part_ref[:, cols] = part_all
+    total_ref[:, cols] = total_all
 
 
 def attend_block(query_ref, key_of, value_of, bias_of, mix_ref, carry_ref, head_size, diagonal):
@@ -332,65 +372,240 @@
     return jnp.where(step <= 2 * near, swing, rest)
 
 
-def layer_kernel(
-    own_ref,
-    stream_ref,
-    gate_ref,
-    up_ref,
-    down_ref,
-    out_ref,
-    rows_buf,
-    pair_w,
-    down_w,
-    hidden,
-    parts,
-    pair_recv,
-    x_far,
-    y_far,
-    x_near,
-    y_near,
-    x_last,
-    y_last,
-    totals,
-    z_recv,
-    local_sem,
-    weight_sems,
-    send_sems,
-    z_got,
-    x_got,
-    y_got,
-    far_got,
-    side_got,
-    pair_got,
-    cross_got,
-    z_sum_got,
-):
+def layer_kernel(names, head_size, *refs):
+    at = types.SimpleNamespace(**dict(zip(names, refs)), head_size=head_size)
     place = Places()
     depth, core, own_z = place.depth, place.core, place.z
-    rows, width = out_ref.shape
-    wide = own_ref.shape[1]
+    rows, width = at.out.shape
     count = 8 * rows
     half = width // 2
-    cut = wide // 256 * 128
+    hidden_width = at.hidden.shape[1]
+    tile = 128
+    sends = Sends(at.send_sems)
+    planes = [plane_order(own_z, depth, step) for step in range(depth)]
+
+    def wait_for(target, sem):
+        remote(target, target, at.send_sems.at[0], sem, place.partner).wait_recv()
+
+    attention_copies = []
+    pieces = []
+    for group in range(at.pack.shape[1]):
+        cols = pl.ds(group * 128, 128)
+        pieces.append((at.keys.at[:, cols], at.pack.at[place.sp, group, 0]))
+        pieces.append((at.values.at[:, cols], at.pack.at[place.sp, group, 1]))
+    for index, (source, target) in enumerate(
+        pieces
+        + [
+            (at.queries, at.query_buf),
+            (at.out_weight, at.out_w),
+            (at.residual, at.base),
+        ]
+    ):
+        copy = pltpu.make_async_copy(source, target, at.copy_sems.at[index])
+        copy.start()
+        attention_copies.append(copy)
+    expert_copies = []
+    for index in range(hidden_width // tile):
+        for which, source in enumerate((at.gate, at.up)):
+            expert_copies.append(
+                pltpu.make_async_copy(
+                    source.at[:, pl.ds(index * tile, tile)],
+                    at.pair_w.at[:, pl.ds((2 * index + which) * tile, tile)],
+                    at.weight_sems.at[len(expert_copies)],
+                )
+            )
+    expert_copies.append(
+        pltpu.make_async_copy(at.down, at.down_w, at.weight_sems.at[len(expert_copies)])
+    )
+    for copy in expert_copies:
+        copy.start()
+    place.meet(True)
+    attention_stage(at, place, sends, wait_for, attention_copies)
+    share_stage(at, place, sends, wait_for, planes)
+    expert_stage(at, place, sends, wait_for, planes, expert_copies)
+    sends.finish()
+
+
+def down_rows(row, rows):
+    lanes = row.shape[1]
+    row_at = lax.broadcasted_iota(jnp.int32, (rows, lanes), 0)
+    lane_at = lax.broadcasted_iota(jnp.int32, (rows, lanes), 1)
+    return jnp.sum(jnp.where(row_at == lane_at, row, 0.0), axis=1, keepdims=True)
+
+
+def attention_stage(at, place, sends, wait_for, copies):
+    pack, biases, routes = at.pack, at.biases, at.routes
+    groups, seq, lanes = pack.shape[1], pack.shape[3], pack.shape[4]
+    size = at.head_size
+    heads = groups * lanes // size
+    own = place.sp
+
+    def piece(block, group):
+        return pack.at[block, group]
+
+    for group in range(groups):
+        copies[2 * group].wait()
+        copies[2 * group + 1].wait()
+        source = piece(own, group)
+        sends.start(source, source, at.pack_x.at[own, group], place.x_next)
+        sends.start(source, source, at.pack_y.at[own, group], place.y_next)
+    biases[own, :heads, :] = at.key_bias[...].astype(jnp.float32)
+    choice, amount = at.choice[...], at.amount[...]
+    rows = choice.shape[1]
+    routes[place.z, place.core, own] = jnp.zeros((8, lanes), jnp.float32)
+    for expert in range(4):
+        chosen = jnp.where(choice == expert, amount, 0.0)
+        total = jnp.sum(chosen, axis=0, keepdims=True)
+        routes[place.z, place.core, own, expert : expert + 1, :rows] = total
+    mine = routes.at[place.z, place.core, own]
+    for target, sem in ((biases.at[own], 0), (mine, 1)):
+        sends.start(target, target, at.small_x.at[own, sem], place.x_next)
+        sends.start(target, target, at.small_y.at[own, sem], place.y_next)
+    row_at = lax.broadcasted_iota(jnp.int32, (seq, seq), 0)
+    col_at = lax.broadcasted_iota(jnp.int32, (seq, seq), 1)
+    later = at.later
+    later[...] = jnp.where(row_at > col_at, 1.0, 0.0).astype(jnp.bfloat16)
+    copies[2 * groups].wait()
+
+    def visit(block, group, diagonal):
+        attend(
+            at.query_buf,
+            lambda cols: pack[block, group, 0],
+            lambda cols: pack[block, group, 1],
+            lambda head: biases[block, head : head + 1, :],
+            later,
+            at.part.at[block],
+            at.total.at[block],
+            size,
+            diagonal,
+            group,
+        )
+
+    def earlier(block, group):
+        @pl.when(block < own)
+        def run():
+            visit(block, group, False)
+
+    across, along, far = place.across, place.along, place.far
+    for group in range(groups):
+        visit(own, group, True)
+    for group in range(groups):
+        from_x, from_y = piece(across, group), piece(along, group)
+        wait_for(from_x, at.pack_x.at[across, group])
+        if group < groups // 2:
+            sends.start(from_x, from_x, at.pack_far.at[group], place.y_next)
+        wait_for(from_y, at.pack_y.at[along, group])
+        if group >= groups // 2:
+            sends.start(from_y, from_y, at.pack_far.at[group], place.x_next)
+        if group == 0:
+            for target, sem in ((biases, 0), (routes.at[place.z, place.core], 1)):
+                wait_for(target.at[across], at.small_x.at[across, sem])
+                wait_for(target.at[along], at.small_y.at[along, sem])
+                sends.start(
+                    target.at[across], target.at[across], at.small_far.at[sem], place.y_next
+                )
+        earlier(across, group)
+        earlier(along, group)
+    for sem, target in enumerate((biases, routes.at[place.z, place.core])):
+        wait_for(target.at[far], at.small_far.at[sem])
+    mine = routes.at[place.z, place.core]
+    sends.start(mine, mine, at.route_side.at[place.z], place.partner)
+    for shift in range(1, place.depth):
+        sends.start(mine, mine, at.route_z.at[place.z], place.z_device(shift))
+    for group in range(groups):
+        wait_for(piece(far, group), at.pack_far.at[group])
+        earlier(far, group)
+    for shift in range(1, place.depth):
+        other = place.z_peer(shift)
+        got = routes.at[other, place.core]
+        wait_for(got, at.route_z.at[other])
+        sends.start(got, got, at.route_side.at[other], place.partner)
+    part, total = at.part, at.total
+
+    def join(step, nothing):
+        block = own - 1 - step
+        part[own] = part[own] + jnp.exp(total[own]) * part[block]
+        total[own] = total[own] + total[block]
+        return nothing
+
+    lax.fori_loop(0, own, join, 0)
+    lane_head = lax.broadcasted_iota(jnp.int32, (1, lanes), 1) // size
+    for group in range(groups):
+        cols = slice(group * lanes, (group + 1) * lanes)
+        mixture = part[own, :, cols]
+        squares = mixture * mixture
+        scaled = mixture
+        for inner in range(lanes // size):
+            chosen = lane_head == inner
+            mean = jnp.sum(jnp.where(chosen, squares, 0.0), axis=1, keepdims=True) / size
+            scaled = jnp.where(chosen, mixture * lax.rsqrt(mean + epsilon), scaled)
+        first = group * (lanes // size)
+        gains = [at.head_gain[first + inner : first + inner + 1, :] for inner in range(lanes // size)]
+        gain = jnp.concatenate(gains, axis=1)
+        at.attended[:, cols] = (scaled * gain).astype(jnp.bfloat16)
+    copies[-2].wait()
+    copies[-1].wait()
+
+
+def share_stage(at, place, sends, wait_for, planes):
+    rows, width = at.out.shape
+    depth, core = place.depth, place.core
+    shares, pair, z_recv = at.shares, at.share_pair, at.share_z
+    tile = 512
+    for start in range(0, width, tile):
+        cols = slice(start, start + tile)
+        share = jnp.dot(
+            at.attended[...], at.out_w[:, cols], preferred_element_type=jnp.float32
+        ).astype(jnp.bfloat16)
+        for z in range(depth):
+            for side in range(2):
+                low = (2 * z + side) * rows
+                shares[side, z, :, cols] = share[low : low + rows]
+    order = planes[1:][::-1] + planes[:1]
+    for plane in order:
+        sends.start(
+            shares.at[1 - core, plane], pair.at[plane], at.share_side.at[plane], place.partner
+        )
+    for index, plane in enumerate(order):
+        wait_for(pair.at[plane], at.share_side.at[plane])
+        total = shares[core, plane].astype(jnp.float32) + pair[plane].astype(jnp.float32)
+        if index < depth - 1:
+            shares[core, plane] = total.astype(jnp.bfloat16)
+            sends.start(
+                shares.at[core, plane],
+                z_recv.at[place.z],
+                at.share_got.at[place.z],
+                (place.sp, plane * 2 + core),
+            )
+    total = total + at.base[...].astype(jnp.float32)
+    for plane in planes[1:]:
+        wait_for(z_recv.at[plane], at.share_got.at[plane])
+        total = total + z_recv[plane].astype(jnp.float32)
+    stream = total.astype(jnp.bfloat16)
+    at.stream[...] = stream
+    normed = rms_scaled(stream.astype(jnp.float32)) * at.norm_gain[...]
+    at.normed[...] = normed.astype(jnp.bfloat16)
+    for plane in planes:
+        side = at.routes.at[plane, 1 - core]
+        wait_for(side, at.route_side.at[plane])
+
+
+def expert_stage(at, place, sends, wait_for, planes, copies):
+    depth, core, own_z = place.depth, place.core, place.z
+    out_ref, own_ref, stream_ref = at.out, at.normed, at.stream
+    rows_buf, pair_w, down_w, hidden = at.rows_buf, at.pair_w, at.down_w, at.hidden
+    parts, pair_recv, totals, z_recv = at.parts, at.pair_recv, at.totals, at.z_recv
+    x_far, y_far, x_near, y_near = at.x_far, at.y_far, at.x_near, at.y_near
+    x_last, y_last, routes = at.x_last, at.y_last, at.routes
+    local_sem, z_got, x_got, y_got = at.local_sem, at.z_got, at.x_got, at.y_got
+    far_got, side_got, pair_got = at.far_got, at.side_got, at.pair_got
+    cross_got, z_sum_got = at.cross_got, at.z_sum_got
+    rows, width = out_ref.shape
+    count = 8 * rows
+    half = width // 2
     hidden_width = hidden.shape[1]
     tile = 128
-    copies = []
-    for index in range(hidden_width // tile):
-        for which, source in enumerate((gate_ref, up_ref)):
-            copies.append(
-                pltpu.make_async_copy(
-                    source.at[:, pl.ds(index * tile, tile)],
-                    pair_w.at[:, pl.ds((2 * index + which) * tile, tile)],
-                    weight_sems.at[len(copies)],
-                )
-            )
-    copies.append(pltpu.make_async_copy(down_ref, down_w, weight_sems.at[len(copies)]))
-    for copy in copies:
-        copy.start()
-    place.meet(True)
-    sends = Sends(send_sems)
-    planes = [plane_order(own_z, depth, step) for step in range(depth)]
-    front, back = pl.ds(0, cut), pl.ds(cut, wide - cut)
+    front, back = pl.ds(0, half), pl.ds(half, half)
     left, right = pl.ds(0, half), pl.ds(half, half)
     z_up = (place.sp, (own_z + 1) * 2 + core)
     z_down = (place.sp, (own_z - 1) * 2 + core)
@@ -398,9 +613,6 @@
 
     def slot(step, seq):
         return rows_buf.at[planes[step], core, seq]
-
-    def wait_for(target, sem):
-        remote(target, target, send_sems.at[0], sem, place.partner).wait_recv()
 
     def to_partner(step, seq, source=None):
         target = slot(step, seq)
@@ -451,41 +663,43 @@
         for seq in (place.sp, place.across, place.along, place.far):
             wait_for(rows_buf.at[plane, 1 - core, seq], side_got.at[plane, seq])
 
-    def compute(step):
+    def open_tiles(step, low, high):
         plane = planes[step]
-
-        def open_tile(index, nothing):
-            spot = pl.multiple_of(index * 2 * tile, 2 * tile)
-            block = rows_buf[plane, :, :, :, :width].reshape(count, width)
+        pieces = []
+        for side in range(2):
+            for seq in range(4):
+                row = routes[plane, side, seq, pl.ds(place.sp, 1), :]
+                pieces.append(down_rows(row, rows))
+        weight = jnp.concatenate(pieces, axis=0)
+        block = rows_buf[plane].reshape(count, width)
+        for index in range(low, high):
             both = jnp.dot(
-                block, pair_w[:, pl.ds(spot, 2 * tile)], preferred_element_type=jnp.float32
+                block,
+                pair_w[:, 2 * index * tile : 2 * (index + 1) * tile],
+                preferred_element_type=jnp.float32,
             )
             gate_part, up_part = both[:, :tile], both[:, tile:]
             value = gate_part / (1.0 + jnp.exp(-gate_part)) * up_part
-            hidden[:, pl.ds(pl.multiple_of(index * tile, tile), tile)] = value.astype(jnp.bfloat16)
-            return nothing
-
-        lax.fori_loop(0, hidden_width // tile, open_tile, 0)
-        lane = lax.broadcasted_iota(jnp.int32, (count, tile), 1)
-        extra = rows_buf[plane, :, :, :, width:].reshape(count, tile).astype(jnp.float32)
-        mine = jnp.logical_or(lane == place.sp, lane == place.sp + 4)
-        weight = jnp.sum(jnp.where(mine, extra, 0.0), axis=1, keepdims=True)
-
-        def down_tile(index, nothing):
-            spot = pl.ds(pl.multiple_of(index * 2 * tile, 2 * tile), 2 * tile)
-            share = jnp.dot(hidden[...], down_w[:, spot], preferred_element_type=jnp.float32)
-            share = jnp.where(weight > 0.0, weight * share, 0.0).astype(jnp.bfloat16)
-            parts[step, :, :, :, spot] = share.reshape(2, 4, rows, 2 * tile)
-            return nothing
-
-        lax.fori_loop(0, width // (2 * tile), down_tile, 0)
+            value = jnp.where(weight > 0.0, weight * value, 0.0)
+            hidden[:, index * tile : (index + 1) * tile] = value.astype(jnp.bfloat16)
+
+    def down_half(step, side):
+        spot = right if side else left
+        share = jnp.dot(hidden[...], down_w[:, spot], preferred_element_type=jnp.float32)
+        parts[step, :, :, :, spot] = share.astype(jnp.bfloat16).reshape(2, 4, rows, half)
         sends.start(
-            parts.at[step, 1 - core], pair_recv.at[step], pair_got.at[step], place.partner
+            parts.at[step, 1 - core, :, :, spot],
+            pair_recv.at[step, :, :, spot],
+            pair_got.at[step, side],
+            place.partner,
         )
 
-    def first_sum(step):
-        wait_for(pair_recv.at[step], pair_got.at[step])
+    def pair_sum(step):
+        for side, spot in enumerate((left, right)):
+            wait_for(pair_recv.at[step, :, :, spot], pair_got.at[step, side])
         add_into(parts.at[step, core], parts.at[step, core], pair_recv.at[step])
+
+    def first_sends(step):
         mine = parts.at[step, core]
         got = cross_got.at[step]
         sends.start(mine.at[place.far, :, left], x_far.at[step], got.at[0], place.x_next)
@@ -536,86 +750,139 @@
 
     local = pltpu.make_async_copy(own_ref, slot(0, place.sp), local_sem)
     local.start()
+    tiles = hidden_width // tile
+    some = (tiles + 1) // 2
     own(0)
     own(1)
     relay(0)
-    for step in range(2, depth):
-        own(step)
-        far(step - 2)
-        relay(step - 1)
+    own(2)
+    far(0)
+    relay(1)
     for copy in copies:
         copy.wait()
     local.wait()
-    order = list(range(1, depth)) + [0]
-    for index, step in enumerate(order):
-        if index == 1:
-            relay(depth - 1)
-        if step == depth - 2:
-            far(depth - 2)
-        if step == depth - 1:
-            far(depth - 1)
+    last = depth - 1
+    for step in range(depth):
+        if step > 0:
+            far(step)
         ready(step)
-        compute(step)
-        if index >= 1:
-            second_sum(order[index - 1])
-        if index >= 2:
-            third_sum(order[index - 2])
-        first_sum(step)
-    second_sum(order[-1])
-    third_sum(order[-2])
-    third_sum(order[-1])
-    sends.finish()
-
-
-def expert_layer(own_rows, stream, gate_matrix, up_matrix, down_matrix):
-    rows, width = stream.shape
-    wide = own_rows.shape[1]
+        open_tiles(step, 0, some)
+        if step + 3 <= last:
+            own(step + 3)
+        if step == 1:
+            pair_sum(0)
+        if step >= 2:
+            pair_sum(step - 1)
+            first_sends(step - 1)
+        open_tiles(step, some, tiles)
+        if step >= 3:
+            third_sum(step - 2)
+        down_half(step, 0)
+        if step + 2 <= last:
+            relay(step + 2)
+        down_half(step, 1)
+        if step >= 2:
+            second_sum(step - 1)
+    pair_sum(last)
+    first_sends(last)
+    first_sends(0)
+    third_sum(last - 1)
+    second_sum(last)
+    second_sum(0)
+    third_sum(last)
+    third_sum(0)
+
+
+def layer(arrays, held, head_size):
+    at = types.SimpleNamespace(**arrays)
+    rows, width = at.residual.shape
+    seq, part_width = at.queries.shape
+    hidden_width = at.gate.shape[1]
     depth = lax.axis_size("tp") // 2
-    hidden_width = gate_matrix.shape[1]
+    groups = part_width // 128
     vmem = pl.BlockSpec(memory_space=pltpu.VMEM)
     anywhere = pl.BlockSpec(memory_space=pl.ANY)
 
     def room(*shape):
         return pltpu.VMEM(shape, jnp.bfloat16)
 
+    def wide_room(*shape):
+        return pltpu.VMEM(shape, jnp.float32)
+
     def sems(*shape):
         return pltpu.SemaphoreType.DMA(shape)
 
-    half = [room(depth, rows, width // 2)] * 6
-    total_sends = depth * (5 + 4 + 1 + 1 + 4 + 2) + depth - 1
+    half = room(depth, rows, width // 2)
+    total_sends = depth * (5 + 4 + 1 + 2 + 4 + 2) + depth - 1
+    total_sends = total_sends + 3 * groups + 6 + 1 + 2 * (depth - 1) + 2 * depth - 1
+    scratch = dict(
+        pack=room(4, groups, 2, seq, 128),
+        query_buf=room(seq, part_width),
+        out_w=room(part_width, width),
+        base=room(rows, width),
+        biases=wide_room(4, 8, seq),
+        routes=wide_room(depth, 2, 4, 8, 128),
+        later=room(seq, seq),
+        part=wide_room(4, seq, part_width),
+        total=wide_room(4, seq, part_width),
+        attended=room(seq, part_width),
+        shares=room(2, depth, rows, width),
+        share_pair=room(depth, rows, width),
+        share_z=room(depth, rows, width),
+        stream=room(rows, width),
+        normed=room(rows, width),
+        rows_buf=room(depth, 2, 4, rows, width),
+        pair_w=room(width, 2 * hidden_width),
+        down_w=room(hidden_width, width),
+        hidden=room(8 * rows, hidden_width),
+        parts=room(depth, 2, 4, rows, width),
+        pair_recv=room(depth, 4, rows, width),
+        x_far=half,
+        y_far=half,
+        x_near=half,
+        y_near=half,
+        x_last=half,
+        y_last=half,
+        totals=room(depth, rows, width),
+        z_recv=room(depth, rows, width),
+        send_sems=sems(total_sends),
+        copy_sems=sems(2 * groups + 3),
+        weight_sems=sems(2 * (hidden_width // 128) + 1),
+        pack_x=sems(4, groups),
+        pack_y=sems(4, groups),
+        pack_far=sems(groups),
+        small_x=sems(4, 2),
+        small_y=sems(4, 2),
+        small_far=sems(2),
+        route_side=sems(depth),
+        route_z=sems(depth),
+        share_side=sems(depth),
+        share_got=sems(depth),
+        local_sem=pltpu.SemaphoreType.DMA,
+        z_got=sems(depth),
+        x_got=sems(depth),
+        y_got=sems(depth),
+        far_got=sems(depth, 2),
+        side_got=sems(depth, 4),
+        pair_got=sems(depth, 2),
+        cross_got=sems(depth, 6),
+        z_sum_got=sems(depth),
+    )
+    names = list(arrays) + ["out"] + list(scratch)
+
+    def body(*refs):
+        layer_kernel(names, head_size, *refs)
+
     return pl.pallas_call(
-        layer_kernel,
+        body,
         out_shape=jax.ShapeDtypeStruct((rows, width), jnp.bfloat16),
-        in_specs=[vmem, vmem, anywhere, anywhere, anywhere],
+        in_specs=[anywhere] * held + [vmem] * (len(arrays) - held),
         out_specs=vmem,
-        scratch_shapes=[
-            room(depth, 2, 4, rows, wide),
-            room(width, 2 * hidden_width),
-            room(hidden_width, width),
-            room(8 * rows, hidden_width),
-            room(depth, 2, 4, rows, width),
-            room(depth, 4, rows, width),
-        ]
-        + half
-        + [
-            room(depth, rows, width),
-            room(depth, rows, width),
-            pltpu.SemaphoreType.DMA,
-            sems(2 * (hidden_width // 128) + 1),
-            sems(total_sends),
-            sems(depth),
-            sems(depth),
-            sems(depth),
-            sems(depth, 2),
-            sems(depth, 4),
-            sems(depth),
-            sems(depth, 6),
-            sems(depth),
-        ],
+        scratch_shapes=list(scratch.values()),
         compiler_params=pltpu.CompilerParams(
             collective_id=1, has_side_effects=True, vmem_limit_bytes=60 * 2**20
         ),
-    )(own_rows, stream, gate_matrix, up_matrix, down_matrix)
+    )(*arrays.values())
 
 
 def on_device(
@@ -642,20 +909,29 @@
     experts_all = local_experts * seq_devices
     capacity = 4 * rows_own // (head_devices * experts_all)
     dense = capacity >= row_share and seq_devices == 4 and head_devices % 4 == 0
-    dense = dense and local_experts == 1 and head_devices >= 8
+    dense = dense and local_experts == 1 and head_devices >= 8 and experts_all == 4
+    dense = dense and rows_own % 128 == 0 and row_share <= 128 and queries.shape[1] % 256 == 0
     if dense:
-        named = expert_choice[:, :, None] == jnp.arange(experts_all, dtype=jnp.int32)
-        own_weights = jnp.sum(jnp.where(named, expert_weights[:, :, None], 0.0), axis=1)
+        arrays = dict(
+            keys=keys,
+            values=values,
+            queries=queries,
+            out_weight=out_weight,
+            residual=residual,
+            gate=gate_proj[0],
+            up=up_proj[0],
+            down=down_proj[0],
+            key_bias=key_bias.T,
+            head_gain=head_gain,
+            norm_gain=norm_gain.reshape(1, -1),
+            choice=expert_choice.T,
+            amount=expert_weights.T,
+        )
+        return layer(arrays, 8, head_gain.shape[1])
     attended = attention(queries, keys, values, key_bias, head_gain)
     shares = jnp.dot(attended, out_weight, preferred_element_type=jnp.float32)
     stream = scatter_sum(shares.astype(jnp.bfloat16), residual, jnp.bfloat16)
     normed = (rms_scaled(stream.astype(jnp.float32)) * norm_gain).astype(jnp.bfloat16)
-    if dense:
-        high = lax.reduce_precision(own_weights, 8, 7)
-        blank = jnp.zeros((row_share, 128 - 2 * experts_all), jnp.bfloat16)
-        extra = [high.astype(jnp.bfloat16), (own_weights - high).astype(jnp.bfloat16), blank]
-        own_rows = jnp.concatenate([normed] + extra, axis=1)
-        return expert_layer(own_rows, stream, gate_proj[0], up_proj[0], down_proj[0])
     own_slots = expert_choice * capacity + choice_ranks(expert_choice, experts_all)
     wanted = slot_tokens(own_slots, experts_all * capacity, row_share)
     outgoing = jnp.take(normed, wanted, axis=0, mode="fill", fill_value=0)

time: 190 us -> 126 us (0.66)
  waiting for transfers between devices: 23.5 us -> 0 us
  between operations: 13.5 us -> 0.01 us
  Pallas kernels: 137 us -> 124 us
  other arithmetic: 5.93 us -> 0 us
  local copies, waits for them, and re-layouts: 7.47 us -> 1.62 us
    all_gather x1 -> x0, waiting for transfers between devices: 23.5 us -> none  [attention(): gathered = lax.all_gather(packed, 'sp', axis=0)]
    pallas_call x4 -> x1, Pallas kernels: 137 us -> 124 us  [layer(): pl.pallas_call(body, out_shape=jax.ShapeDtypeStruct((rows, width), jnp.bf...]
    reshape x4 -> x0, local copies, waits for them, and re-layouts: 3.38 us -> none  [the longest x1 1.31 us: attention(): head_gain.reshape(1, width)]
    convert_element_type x4 -> x0, other arithmetic: 2.34 us -> none  [the longest x1 1.28 us: attention(): bias_own.astype(jnp.float32)]
  transfers between devices with their start and end apart: 1 -> 0, of which waited for: 1 -> 0; matrix products, arithmetic and copies ran while one was open for 2% -> 0% of each run, Pallas kernels for 4% -> 0%
where the time goes in v2:
time: 126 us
  Pallas kernels  124 us (98%)
  local copies, waits for them, and re-layouts  1.62 us (1%)
    pallas_call x1, Pallas kernels, layer(): pl.pallas_call(body, out_shape=jax.ShapeDtypeStruct((rows, width), jnp.bf...  124 us

profile of v2, /device:TPU:0, one launch (start us, length us, event | category | flops | bytes accessed | tf_op | source)
XLA Modules:
  0.0 125.9 jit_solution(8723122495384186594)
XLA Ops:
  0.0 124.3 %shard_map.127 = bf16[48,2048]{1,0:T(8,128)(2,1)} custom-call(bf16[384,256]{1,0:T(8,128)(2,1)} %refs_0_.1, bf16[384,256]{1,0:T(8,128)(2,1)} %refs_1_.1, bf16[384,256]{1,0:T(8,128)(2,1)} %refs_2_.1, bf16[256,2048]{1,0:T(8,128)(2,1)} %refs_3_.1, bf16[48,2048]{1,0:T(8,128)(2,1)} %refs_4_.1, bf16[2048,896]{1,0:T(8,128)(2,1)} %bitcast.7, ...), custom_call_target="tpu_custom_call" | custom-call | tf_op jit(solution)/shard_map/pallas_call | solution.py:876
  124.3 1.6 %copy.15 = bf16[48,2048]{1,0:T(8,128)(2,1)} copy(bf16[48,2048]{1,0:T(8,128)(2,1)} %shard_map.127) | data formatting | bytes 393216

commit v3 on v2

--- a/solution.py
+++ b/solution.py
@@ -605,7 +605,18 @@
     half = width // 2
     hidden_width = hidden.shape[1]
     tile = 128
-    front, back = pl.ds(0, half), pl.ds(half, half)
+    main = width - width // 8
+    slim = pl.ds(main, width - main)
+
+    def first_part(step):
+        return pl.ds(0, half if step == 0 else main // 2)
+
+    def second_part(step):
+        return pl.ds(half, half) if step == 0 else pl.ds(main // 2, main // 2)
+
+    def body_part(step):
+        return pl.ds(0, width if step == 0 else main)
+
     left, right = pl.ds(0, half), pl.ds(half, half)
     z_up = (place.sp, (own_z + 1) * 2 + core)
     z_down = (place.sp, (own_z - 1) * 2 + core)
@@ -614,54 +625,85 @@
     def slot(step, seq):
         return rows_buf.at[planes[step], core, seq]
 
-    def to_partner(step, seq, source=None):
-        target = slot(step, seq)
-        sends.start(
-            target if source is None else source,
-            target,
-            side_got.at[planes[step], seq],
-            place.partner,
-        )
-
-    def own(step):
+    inner = jnp.logical_and(has_up, has_down)
+    outer = jnp.logical_not(inner)
+
+    def both_of(first, second):
+        return first if second is None else jnp.logical_and(first, second)
+
+    def to_partner(step, seq):
+        target = slot(step, seq).at[:, body_part(step)]
+        sends.start(target, target, side_got.at[planes[step], seq], place.partner)
+
+    def own(step, when=None):
         plane = planes[step]
         target = slot(step, place.sp)
-        source = own_ref
+        source, go_up, go_down = own_ref, has_up, has_down
         if step > 0:
-            wait_for(target, z_got.at[plane])
             source = target
             go_up = jnp.logical_and(has_up, plane < own_z)
             go_down = jnp.logical_and(has_down, plane > own_z)
-        else:
-            go_up, go_down = has_up, has_down
-        if depth > 1:
-            sends.start(source, target, z_got.at[plane], z_up, go_up)
-            sends.start(source, target, z_got.at[plane], z_down, go_down)
-        sends.start(source, target, x_got.at[plane], place.x_next)
-        sends.start(source, target, y_got.at[plane], place.y_next)
-        to_partner(step, place.sp, source)
+            if when is None:
+                wait_for(target, z_got.at[plane])
+            else:
+                pl.when(when)(lambda: wait_for(target, z_got.at[plane]))
+        sends.start(source, target, z_got.at[plane], z_up, both_of(go_up, when))
+        sends.start(source, target, z_got.at[plane], z_down, both_of(go_down, when))
+        part = body_part(step)
+        near, there = source.at[:, part], target.at[:, part]
+        sends.start(near, there, x_got.at[plane], place.x_next, when)
+        sends.start(near, there, y_got.at[plane], place.y_next, when)
+        sends.start(source, target, side_got.at[plane, place.sp], place.partner, when)
+
+    def slim_out(seq):
+        piece = slot(0, seq).at[:, slim]
+        for plane in planes[1:]:
+            device = (place.sp, plane * 2 + core)
+            sends.start(piece, piece, at.slim_got.at[own_z, seq], device)
 
     def relay(step):
         plane = planes[step]
         across, along = slot(step, place.across), slot(step, place.along)
-        wait_for(across, x_got.at[plane])
+        front, back = first_part(step), second_part(step)
+        part = body_part(step)
+        wait_for(across.at[:, part], x_got.at[plane])
         sends.start(across.at[:, front], across.at[:, front], far_got.at[plane, 0], place.y_next)
-        wait_for(along, y_got.at[plane])
+        wait_for(along.at[:, part], y_got.at[plane])
         sends.start(along.at[:, back], along.at[:, back], far_got.at[plane, 1], place.x_next)
         to_partner(step, place.across)
         to_partner(step, place.along)
+        if step == 0:
+            slim_out(place.across)
+            slim_out(place.along)
 
     def far(step):
         plane = planes[step]
         target = slot(step, place.far)
-        wait_for(target.at[:, front], far_got.at[plane, 0])
-        wait_for(target.at[:, back], far_got.at[plane, 1])
+        wait_for(target.at[:, first_part(step)], far_got.at[plane, 0])
+        wait_for(target.at[:, second_part(step)], far_got.at[plane, 1])
         to_partner(step, place.far)
+        if step == 0:
+            slim_out(place.far)
+
+    def slims(step):
+        plane = planes[step]
+        for seq in (place.across, place.along, place.far):
+            piece = slot(step, seq).at[:, slim]
+            wait_for(piece, at.slim_got.at[plane, seq])
+            sends.start(piece, piece, at.slim_side.at[plane, seq], place.partner)
 
     def ready(step):
         plane = planes[step]
         for seq in (place.sp, place.across, place.along, place.far):
-            wait_for(rows_buf.at[plane, 1 - core, seq], side_got.at[plane, seq])
+            target = rows_buf.at[plane, 1 - core, seq]
+            if step == 0:
+                wait_for(target, side_got.at[plane, seq])
+        if step > 0:
+            wait_for(rows_buf.at[plane, 1 - core, place.sp], side_got.at[plane, place.sp])
+            for seq in (place.across, place.along, place.far):
+                target = rows_buf.at[plane, 1 - core, seq]
+                wait_for(target.at[:, body_part(step)], side_got.at[plane, seq])
+                wait_for(target.at[:, slim], at.slim_side.at[plane, seq])
 
     def open_tiles(step, low, high):
         plane = planes[step]
@@ -763,32 +805,41 @@
     local.wait()
     last = depth - 1
     for step in range(depth):
-        if step > 0:
-            far(step)
         ready(step)
         open_tiles(step, 0, some)
         if step + 3 <= last:
-            own(step + 3)
+            own(step + 3, inner)
         if step == 1:
             pair_sum(0)
+            first_sends(0)
         if step >= 2:
             pair_sum(step - 1)
             first_sends(step - 1)
         open_tiles(step, some, tiles)
+        if step >= 1 and step + 2 <= last:
+            relay(step + 2)
         if step >= 3:
             third_sum(step - 2)
         down_half(step, 0)
-        if step + 2 <= last:
-            relay(step + 2)
-        down_half(step, 1)
+        if step == 0:
+            down_half(step, 1)
+            for later in range(3, depth):
+                own(later, outer)
+            relay(2)
+        if step < last:
+            far(step + 1)
+        if step > 0:
+            down_half(step, 1)
+        if step < last:
+            slims(step + 1)
         if step >= 2:
+            if step == 2:
+                second_sum(0)
             second_sum(step - 1)
     pair_sum(last)
     first_sends(last)
-    first_sends(0)
     third_sum(last - 1)
     second_sum(last)
-    second_sum(0)
     third_sum(last)
     third_sum(0)
 
@@ -813,8 +864,7 @@
         return pltpu.SemaphoreType.DMA(shape)
 
     half = room(depth, rows, width // 2)
-    total_sends = depth * (5 + 4 + 1 + 2 + 4 + 2) + depth - 1
-    total_sends = total_sends + 3 * groups + 6 + 1 + 2 * (depth - 1) + 2 * depth - 1
+    total_sends = 48 * depth + 3 * groups + 16
     scratch = dict(
         pack=room(4, groups, 2, seq, 128),
         query_buf=room(seq, part_width),
@@ -864,6 +914,8 @@
         y_got=sems(depth),
         far_got=sems(depth, 2),
         side_got=sems(depth, 4),
+        slim_got=sems(depth, 4),
+        slim_side=sems(depth, 4),
         pair_got=sems(depth, 2),
         cross_got=sems(depth, 6),
         z_sum_got=sems(depth),

time: 126 us -> 122 us (0.968)
  Pallas kernels: 124 us -> 121 us
    pallas_call x1, Pallas kernels: 124 us -> 121 us  [layer(): pl.pallas_call(body, out_shape=jax.ShapeDtypeStruct((rows, width), jnp.bf...]
where the time goes in v3:
time: 122 us
  Pallas kernels  121 us (99%)
  local copies, waits for them, and re-layouts  1.62 us (1%)
    pallas_call x1, Pallas kernels, layer(): pl.pallas_call(body, out_shape=jax.ShapeDtypeStruct((rows, width), jnp.bf...  121 us

profile of v3, /device:TPU:0, one launch (start us, length us, event | category | flops | bytes accessed | tf_op | source)
XLA Modules:
  0.0 122.1 jit_solution(16133632232886540212)
XLA Ops:
  0.0 120.5 %shard_map.127 = bf16[48,2048]{1,0:T(8,128)(2,1)} custom-call(bf16[384,256]{1,0:T(8,128)(2,1)} %refs_0_.1, bf16[384,256]{1,0:T(8,128)(2,1)} %refs_1_.1, bf16[384,256]{1,0:T(8,128)(2,1)} %refs_2_.1, bf16[256,2048]{1,0:T(8,128)(2,1)} %refs_3_.1, bf16[48,2048]{1,0:T(8,128)(2,1)} %refs_4_.1, bf16[2048,896]{1,0:T(8,128)(2,1)} %bitcast.7, ...), custom_call_target="tpu_custom_call" | custom-call | tf_op jit(solution)/shard_map/pallas_call | solution.py:928
  120.5 1.6 %copy.15 = bf16[48,2048]{1,0:T(8,128)(2,1)} copy(bf16[48,2048]{1,0:T(8,128)(2,1)} %shard_map.127) | data formatting | bytes 393216
